TPU v7x, 32 devices: a whole 2x2x4 slice. The times are simulated.
32 devices in a mesh: sp: 8 (over z, y), tp: 4 (over x, core).
Axes of the slice: x: 2, y: 2, z: 4, core: 2. Of those that a mesh axis runs over, the one named last changes fastest.
Arguments:
- resid: bfloat16 [6144, 2048], P(('sp', 'tp')), may hold values from -6 to 6
- query: bfloat16 [6144, 1024], P('sp', 'tp'), may hold values from -6 to 6
- keys: bfloat16 [6144, 1024], P('sp', 'tp'), may hold values from -6 to 6
- values: bfloat16 [6144, 1024], P('sp', 'tp'), may hold values from -6 to 6
- out_gate: bfloat16 [6144, 1024], P(('sp', 'tp')), may hold values from -6 to 6
- forget_pre: float32 [4, 6144], P('tp', 'sp'), may hold values from 0 to 16
- input_pre: float32 [4, 6144], P('tp', 'sp'), may hold values from -4 to 130
- head_gain: float32 [1024], replicated, may hold values from 0.1 to 1.9
- out_proj: bfloat16 [1024, 2048], replicated, may hold values from -0.1875 to 0.1875
- ffn_gain: float32 [2048], replicated, may hold values from 0.1 to 1.9
- routes: int32 [6144, 2], P(('sp', 'tp')), may hold values from 0 to 7, all different within a row; in each aligned block of 96 rows (0 to 95, 96 to 191, ...) at most 48 rows name the same one
- route_scores: float32 [6144, 2], P(('sp', 'tp')), may hold values from 0.1 to 1
- w_gate: bfloat16 [8, 2048, 512], P('sp'), may hold values from -0.125 to 0.125
- w_up: bfloat16 [8, 2048, 512], P('sp'), may hold values from -0.125 to 0.125
- w_down: bfloat16 [8, 512, 2048], P('sp'), may hold values from -0.25 to 0.25
Outputs:
- layer_out: bfloat16 [6144, 2048], P(('sp', 'tp'))
Inputs may be any that keep to these rules, and one draw needn't show every extreme that they name: `routes`: each row names 2 different experts; in each aligned block of 96 rows no expert is named by more than 48 rows, a bound that some block reaches.
All inputs are finite; a program needn't handle non-finite values.
Results may differ from a plain program's by a relative error of at most 0.0095.
Values may be sent and summed in bfloat16 or wider, within the bound.
No kernel may reach another device: no remote copies, remote signals or barrier semaphores. Data moves between devices by JAX's collectives and lax.ppermute only.
A program may use at most 128 MiB of HBM per device.

v0:
```python
import jax
import jax.numpy as jnp
from jax import lax
from jax.sharding import PartitionSpec as P

BLOCK = 64


EPS = 1e-06
FLOOR_LOG = -1e30
HIGHEST = lax.Precision.HIGHEST


def prefix(part, axis, combine, identity):
    place = lax.axis_index(axis)
    gathered = jax.tree.map(lambda a: lax.all_gather(a, axis), part)
    state = jax.tree.map(lambda a, e: jnp.zeros_like(a) + jnp.asarray(e, a.dtype), part, identity)

    def one(step, state):
        return combine(
            state, jax.tree.map(lambda a: lax.dynamic_index_in_dim(a, step, 0, False), gathered)
        )

    return lax.fori_loop(0, place, one, state)


def block_pass(query, keys, values, log_forget, log_input, state):
    seq_len, head_width = query.shape
    blocks = seq_len // BLOCK
    key_scale = head_width ** (-0.5)
    causal = jnp.tril(jnp.ones((BLOCK, BLOCK), dtype=bool))

    def block_step(state_in, inputs):
        state_mat, state_vec, max_log = state_in
        q_block, k_block, v_block, forget_blk, input_blk = inputs
        cum_log = jnp.cumsum(forget_blk)
        block_total = cum_log[-1]
        log_mat = jnp.where(
            causal, cum_log[:, None] - cum_log[None, :] + input_blk[None, :], -jnp.inf
        )
        inter_log = cum_log + max_log
        row_max = jnp.maximum(inter_log, jnp.max(log_mat, axis=1))
        weight_mat = jnp.exp(log_mat - row_max[:, None])
        carry_weight = jnp.exp(inter_log - row_max)
        scores = jnp.dot(q_block, k_block.T, preferred_element_type=jnp.float32) * key_scale
        weights_blk = (scores * weight_mat).astype(jnp.bfloat16)
        q_float = q_block.astype(jnp.float32)
        numerator = carry_weight[:, None] * jnp.dot(
            q_float, state_mat, precision=HIGHEST
        ) + jnp.dot(weights_blk, v_block, preferred_element_type=jnp.float32)
        denominator = carry_weight * jnp.dot(q_float, state_vec, precision=HIGHEST) + jnp.sum(
            weights_blk.astype(jnp.float32), axis=1
        )
        log_keep = block_total - cum_log + input_blk
        new_max = jnp.maximum(block_total + max_log, jnp.max(log_keep))
        keep_weight = jnp.exp(log_keep - new_max)
        decay_now = jnp.exp(block_total + max_log - new_max)
        k_float = k_block.astype(jnp.float32) * key_scale
        state_mat = decay_now * state_mat + jnp.dot(
            (k_float * keep_weight[:, None]).T, v_block.astype(jnp.float32), precision=HIGHEST
        )
        state_vec = decay_now * state_vec + jnp.dot(keep_weight, k_float, precision=HIGHEST)
        return ((state_mat, state_vec, new_max), (numerator, denominator, row_max))

    def to_blocks(array_in):
        return array_in.reshape((blocks, BLOCK) + array_in.shape[1:])

    ignored, outputs = lax.scan(
        block_step,
        state,
        (
            to_blocks(query),
            to_blocks(keys),
            to_blocks(values),
            to_blocks(log_forget),
            to_blocks(log_input),
        ),
    )
    numerator, denominator, row_max = outputs
    return (
        numerator.reshape(seq_len, head_width),
        denominator.reshape(seq_len),
        row_max.reshape(seq_len),
    )


def end_state(keys, values, log_forget, log_input):
    head_width = keys.shape[1]
    cum_log = jnp.cumsum(log_forget)
    block_total = cum_log[-1]
    log_keep = block_total - cum_log + log_input
    max_log = jnp.max(log_keep)
    keep_weight = jnp.exp(log_keep - max_log)
    k_float = keys.astype(jnp.float32) * head_width ** (-0.5)
    state_mat = jnp.dot(
        (k_float * keep_weight[:, None]).T, values.astype(jnp.float32), precision=HIGHEST
    )
    state_vec = jnp.dot(keep_weight, k_float, precision=HIGHEST)
    return (state_mat, state_vec, max_log, block_total)


def join_states(earlier, latter):
    old_mat, old_vec, old_max, old_total = earlier
    new_mat, new_vec, new_max, new_total = latter
    joined_max = jnp.maximum(new_total + old_max, new_max)
    keep_old = jnp.exp(new_total + old_max - joined_max)
    keep_new = jnp.exp(new_max - joined_max)
    joined_mat = keep_old[:, None, None] * old_mat + keep_new[:, None, None] * new_mat
    joined_vec = keep_old[:, None] * old_vec + keep_new[:, None] * new_vec
    return (joined_mat, joined_vec, joined_max, old_total + new_total)


def slot_select(expert_ids, expert_count, capacity):
    flat_ids = expert_ids.reshape(-1)
    one_hot = (flat_ids[:, None] == jnp.arange(expert_count, dtype=jnp.int32)[None, :]).astype(
        jnp.int32
    )
    slot_rank = jnp.sum((jnp.cumsum(one_hot, axis=0) - 1) * one_hot, axis=1)
    target = flat_ids * capacity + slot_rank
    return (
        jnp.arange(expert_count * capacity, dtype=jnp.int32)[:, None] == target[None, :]
    ).astype(jnp.bfloat16)


def run_experts(arrived, w_gate, w_up, w_down, sources):
    local_count = w_gate.shape[0]
    grouped = arrived.reshape(sources, local_count, arrived.shape[1], arrived.shape[2])
    gate_pre = jnp.einsum("pesd,edf->pesf", grouped, w_gate, preferred_element_type=jnp.float32)
    up_pre = jnp.einsum("pesd,edf->pesf", grouped, w_up, preferred_element_type=jnp.float32)
    active = (jax.nn.silu(gate_pre) * up_pre).astype(jnp.bfloat16)
    result = jnp.einsum(
        "pesf,efd->pesd", active, w_down, preferred_element_type=jnp.float32
    ).astype(jnp.bfloat16)
    return result.reshape(arrived.shape)


def shards(
    resid,
    query,
    keys,
    values,
    out_gate,
    forget_pre,
    input_pre,
    head_gain,
    out_proj,
    ffn_gain,
    routes,
    route_scores,
    w_gate,
    w_up,
    w_down,
):
    local_heads = forget_pre.shape[0]
    seq_len = query.shape[0]
    head_width = query.shape[1] // local_heads
    log_forget = jax.nn.log_sigmoid(forget_pre)
    q_heads = query.reshape(seq_len, local_heads, head_width)
    k_heads = keys.reshape(seq_len, local_heads, head_width)
    v_heads = values.reshape(seq_len, local_heads, head_width)
    state_mat, state_vec, max_log, totals = jax.vmap(end_state, in_axes=(1, 1, 0, 0))(
        k_heads, v_heads, log_forget, input_pre
    )
    identity = (
        jnp.zeros((local_heads, head_width, head_width), jnp.float32),
        jnp.zeros((local_heads, head_width), jnp.float32),
        jnp.full((local_heads,), FLOOR_LOG, jnp.float32),
        jnp.zeros((local_heads,), jnp.float32),
    )
    carried = prefix((state_mat, state_vec, max_log, totals), "sp", join_states, identity)
    pass_heads = jax.vmap(block_pass, in_axes=(1, 1, 1, 0, 0, 0), out_axes=(1, 1, 1))
    numerator, denominator, row_max = pass_heads(
        q_heads, k_heads, v_heads, log_forget, input_pre, (identity[0], identity[1], identity[2])
    )
    cum_all = jnp.cumsum(log_forget, axis=1).T + carried[2][None, :]
    joined_max = jnp.maximum(row_max, cum_all)
    keep_own = jnp.exp(row_max - joined_max)
    keep_far = jnp.exp(cum_all - joined_max)
    q_float = q_heads.astype(jnp.float32)
    numerator = keep_own[:, :, None] * numerator + keep_far[:, :, None] * jnp.einsum(
        "lhd,hde->lhe", q_float, carried[0], precision=HIGHEST
    )
    denominator = keep_own * denominator + keep_far * jnp.einsum(
        "lhd,hd->lh", q_float, carried[1], precision=HIGHEST
    )
    row_max = joined_max
    hidden = numerator / jnp.maximum(jnp.abs(denominator), jnp.exp(-row_max))[:, :, None]
    cell_rows = hidden.reshape(seq_len, local_heads * head_width).astype(jnp.bfloat16)
    token_rows = lax.all_to_all(cell_rows, "tp", split_axis=0, concat_axis=1, tiled=True)
    cell_float = token_rows.astype(jnp.float32)
    headed = (
        cell_float
        * lax.rsqrt(jnp.mean(cell_float * cell_float, axis=1, keepdims=True) + EPS)
        * head_gain[None, :]
    )
    gated_out = (headed * jax.nn.sigmoid(out_gate.astype(jnp.float32))).astype(jnp.bfloat16)
    after_mix = resid.astype(jnp.float32) + jnp.dot(
        gated_out, out_proj, preferred_element_type=jnp.float32
    )
    normed_rows = (
        after_mix
        * lax.rsqrt(jnp.mean(after_mix * after_mix, axis=1, keepdims=True) + EPS)
        * ffn_gain[None, :]
    ).astype(jnp.bfloat16)
    row_count = normed_rows.shape[0]
    half_rows = row_count // 2
    route_count = routes.shape[1]
    sources = lax.axis_size("sp")
    expert_count = w_gate.shape[0] * sources
    capacity = max(2, 2 * half_rows * route_count // expert_count)
    selects = [
        slot_select(
            routes[half_idx * half_rows : (half_idx + 1) * half_rows], expert_count, capacity
        )
        for half_idx in range(2)
    ]

    def pack_rows(half_idx):
        selection = (
            selects[half_idx].reshape(expert_count * capacity, half_rows, route_count).sum(axis=2)
        )
        packed = jnp.dot(
            selection,
            normed_rows[half_idx * half_rows : (half_idx + 1) * half_rows],
            preferred_element_type=jnp.float32,
        )
        return packed.astype(jnp.bfloat16).reshape(expert_count, capacity, normed_rows.shape[1])

    send_rows = jnp.concatenate([pack_rows(0), pack_rows(1)], axis=1)
    finished = run_experts(
        lax.all_to_all(send_rows, "sp", split_axis=0, concat_axis=0, tiled=True),
        w_gate,
        w_up,
        w_down,
        sources,
    )
    returned = lax.all_to_all(finished, "sp", split_axis=0, concat_axis=0, tiled=True)
    answers = [returned[:, :capacity], returned[:, capacity:]]
    route_weight = route_scores / jnp.sum(route_scores, axis=1, keepdims=True)
    pieces = []
    for half_idx in range(2):
        gathered = lax.dot_general(
            selects[half_idx],
            answers[half_idx].reshape(expert_count * capacity, -1),
            (((0,), (0,)), ((), ())),
            preferred_element_type=jnp.float32,
        )
        weights_half = route_weight[half_idx * half_rows : (half_idx + 1) * half_rows]
        pieces.append(
            jnp.sum(gathered.reshape(half_rows, route_count, -1) * weights_half[:, :, None], axis=1)
        )
    return (after_mix + jnp.concatenate(pieces, axis=0)).astype(jnp.bfloat16)


def solution(mesh):
    placed = (
        P(("sp", "tp"), None),
        P("sp", "tp"),
        P("sp", "tp"),
        P("sp", "tp"),
        P(("sp", "tp"), None),
        P("tp", "sp"),
        P("tp", "sp"),
        P(),
        P(),
        P(),
        P(("sp", "tp"), None),
        P(("sp", "tp"), None),
        P("sp", None, None),
        P("sp", None, None),
        P("sp", None, None),
    )
    return jax.shard_map(
        shards, mesh=mesh, in_specs=placed, out_specs=P(("sp", "tp"), None), check_vma=False
    )
```

profile of v0, /device:TPU:0, one launch (start us, length us, event | category | flops | bytes accessed | tf_op | source)
XLA Modules:
  0.0 429.5 jit_solution(1679653552651287913)
XLA Ops:
  8.8 2.0 fusion.111
  11.4 2.8 fusion.79
  18.5 136.7 %while.38 = (s32[]{:T(128)}, f32[1,256,256]{2,1,0:T(8,128)S(1)}, f32[1,256]{1,0:T(1,128)S(1)}, f32[1]{0:T(128)}, f32[12,1,64,256]{3,2,1,0:T(8,128)}, /*index=5*/...) while((s32[]{:T(128)}, f32[1,256,256]{2,1,0:T(8,128)S(1)}, ...), condition=%wide.region_5.6_spmd.clone, body=%wide.region_0.5_spmd.clone.sunk | while | flops 105678720 | bytes 1283846 | solution.py:68
  24.5 1.6 fusion.158
  28.3 1.6 convolution_add_fusion.4
  35.9 1.6 fusion.158
  47.3 1.6 fusion.158
  51.1 1.6 convolution_add_fusion.4
  62.5 1.6 convolution_add_fusion.4
  73.8 1.6 convolution_add_fusion.4
  85.2 1.6 convolution_add_fusion.4
  92.9 1.6 fusion.158
  96.6 1.6 convolution_add_fusion.4
  108.0 1.6 convolution_add_fusion.4
  119.4 1.6 convolution_add_fusion.4
  130.8 1.6 convolution_add_fusion.4
  138.4 1.6 fusion.158
  142.2 1.6 convolution_add_fusion.4
  153.6 1.6 convolution_add_fusion.4
  155.2 23.8 %all-reduce.4 = (f32[8]{0:T(128)}, f32[8]{0:T(128)}) all-reduce(f32[8]{0:T(128)S(1)} %bitcast_dynamic-update-slice_fusion, f32[8]{0:T(128)S(1)} %dynamic-update-slice.1), channel_id=1, replica_groups=mesh['sp'=8,'tp'=4] {'sp'}, use_global_device_ids=true, to_apply=%add.2 | all-reduce | flops 16 | bytes 128
  186.8 16.3 %all-gather.2 = f32[8,1,256]{2,1,0:T(1,128)S(1)} all-gather(f32[1,1,256]{2,1,0:T(1,128)S(1)} %convolution_bitcast_fusion.3), channel_id=3, replica_groups=mesh['sp'=8,'tp'=4] {'sp'}, dimensions={0}, use_global_device_ids=true | all-gather | bytes 9216 | tf_op jit(solution)/shard_map/all_gather | solution.py:16
  207.6 1.9 copy.46
  209.5 3.5 all-to-all-start
  213.4 6.9 %all-to-all-done = bf16[4,192,256]{2,1,0:T(8,128)(2,1)S(1)} async-done(((bf16[4,192,256]{2,1,0:T(8,128)(2,1)}), bf16[4,192,256]{2,1,0:T(8,128)(2,1)S(1)}, u32[]{:S(2)}, u32[]{:S(2)}) %all-to-all-start) | async-done | bytes 393248 | tf_op jit(solution)/shard_map/all_to_all | solution.py:189
  221.5 3.5 multiply_reduce_fusion
  227.1 103.0 %all_to_all.20 = bf16[8,96,2048]{2,1,0:T(8,128)(2,1)S(1)} all-to-all(bf16[8,96,2048]{2,1,0:T(8,128)(2,1)S(1)} %pad_maximum_fusion), channel_id=1, replica_groups=mesh['sp'=8,'tp'=4] {'sp'}, dimensions={0} | all-to-all | bytes 6291456 | tf_op jit(solution)/shard_map/all_to_all | solution.py:231
  330.1 1.7 copy-done.3
  331.8 3.0 fusion.60
  334.9 8.2 %convolution_convert_fusion = bf16[8,96,2048]{2,1,0:T(8,128)(2,1)} fusion(bf16[1,512,2048]{2,1,0:T(8,128)(2,1)S(1)} %copy-done, bf16[8,96,2048]{2,1,0:T(8,128)(2,1)} %copy-done.3, bf16[1,2048,512]{2,1,0:T(8,128)(2,1)} %param.32, f32[8,96,512]{2,1,0:T(8,128)} %fusion.60), kind=kOutput, calls=%fused_computation.78 | convolution fusion | flops 3225157632 | bytes 12058624 | tf_op jit(solution)/shard_map/pesf,efd->pesd/dot_general | solution.py:131
  343.0 4.5 %all-to-all-start.2 = ((bf16[8,96,2048]{2,1,0:T(8,128)(2,1)}), bf16[8,96,2048]{2,1,0:T(8,128)(2,1)}, u32[]{:S(2)}, u32[]{:S(2)}) async-start(bf16[8,96,2048]{2,1,0:T(8,128)(2,1)} %convolution_convert_fusion), calls=%async_computation.2 | async-start | bytes 6291456 | tf_op jit(solution)/shard_map/all_to_all | solution.py:237
  348.1 69.2 %all-to-all-done.2 = bf16[8,96,2048]{2,1,0:T(8,128)(2,1)} async-done(((bf16[8,96,2048]{2,1,0:T(8,128)(2,1)}), bf16[8,96,2048]{2,1,0:T(8,128)(2,1)}, u32[]{:S(2)}, u32[]{:S(2)}) %all-to-all-start.2) | async-done | bytes 3145760 | tf_op jit(solution)/shard_map/all_to_all | solution.py:237
  417.3 2.3 fusion.112
  (290 shorter events, 122.3 us)
Async XLA Ops:
  6.5 328.3 %copy-start = (bf16[1,512,2048]{2,1,0:T(8,128)(2,1)S(1)}, bf16[1,512,2048]{2,1,0:T(8,128)(2,1)}, u32[]{:S(2)}) copy-start(bf16[1,512,2048]{2,1,0:T(8,128)(2,1)} %param.33) | copy-start | bytes 6291460
  6.5 197.2 %all-gather.5.cloned.1.call-start = ((), (), s32[]{:S(2)}) async-start(), calls=%async_computation.3 | async-start | bytes 2359296 | tf_op jit(solution)/shard_map/all_gather | solution.py:16
  8.1 10.4 %copy-start.21 = (f32[6]{0:T(128)}, f32[6]{0:T(128)S(1)}, u32[]{:S(2)}) copy-start(f32[6]{0:T(128)S(1)} %slice_bitcast_fusion) | copy-start | bytes 76
  155.2 26.6 %copy-start.20 = (s32[192,2]{0,1:T(2,128)S(1)}, s32[192,2]{0,1:T(2,128)}, u32[]{:S(2)}) copy-start(s32[192,2]{0,1:T(2,128)} %param.29) | copy-start | bytes 4612
  155.2 30.5 %copy-start.4 = (bf16[12,1,64,256]{3,2,1,0:T(8,128)(2,1)S(1)}, bf16[12,1,64,256]{3,2,1,0:T(8,128)(2,1)}, u32[]{:S(2)}) copy-start(bf16[12,1,64,256]{3,2,1,0:T(8,128)(2,1)} %get-tuple-element.533) | copy-start | bytes 1179652
  182.1 1.1 copy-start.10
  183.1 0.6 copy-start.14
  183.8 19.9 %copy-start.6 = (s32[96,2]{1,0:T(8,128)}, s32[96,2]{1,0:T(8,128)S(1)}, u32[]{:S(2)}) copy-start(s32[96,2]{1,0:T(8,128)S(1)} %copy.55) | copy-start | bytes 2308
  183.9 19.8 %copy-start.12 = (s32[192]{0:T(256)}, s32[192]{0:T(256)S(1)}, u32[]{:S(2)}) copy-start(s32[192]{0:T(256)S(1)} %eq.114) | copy-start | bytes 2308
  184.9 18.8 %copy-start.16 = (s32[192]{0:T(256)}, s32[192]{0:T(256)S(1)}, u32[]{:S(2)}) copy-start(s32[192]{0:T(256)S(1)} %fusion.98) | copy-start | bytes 2308
  203.8 1.0 copy-start.5
  207.6 5.4 %copy-start.7 = (s32[96,2]{1,0:T(8,128)S(1)}, s32[96,2]{1,0:T(8,128)}, u32[]{:S(2)}) copy-start(s32[96,2]{1,0:T(8,128)} %copy-done.6) | copy-start | bytes 2308
  207.6 5.4 %copy-start.8 = (s32[96,2]{1,0:T(8,128)S(1)}, s32[96,2]{1,0:T(8,128)}, u32[]{:S(2)}) copy-start(s32[96,2]{1,0:T(8,128)} %reduce_sum.106) | copy-start | bytes 2308
  207.6 5.4 %copy-start.9 = (s32[96,2]{1,0:T(8,128)S(1)}, s32[96,2]{1,0:T(8,128)}, u32[]{:S(2)}) copy-start(s32[96,2]{1,0:T(8,128)} %multiply_add_fusion.1) | copy-start | bytes 2308
  209.5 10.8 %all-to-all-start = ((bf16[4,192,256]{2,1,0:T(8,128)(2,1)}), bf16[4,192,256]{2,1,0:T(8,128)(2,1)S(1)}, u32[]{:S(2)}, u32[]{:S(2)}) async-start(bf16[4,192,256]{2,1,0:T(8,128)(2,1)} %bitcast.29), calls=%async_computation | async-start | bytes 786432 | tf_op jit(solution)/shard_map/all_to_all | solution.py:189
  213.4 7.3 %copy-start.24 = (bf16[192,1024]{1,0:T(8,128)(2,1)S(1)}, bf16[192,1024]{1,0:T(8,128)(2,1)}, u32[]{:S(2)}) copy-start(bf16[192,1024]{1,0:T(8,128)(2,1)} %param.23) | copy-start | bytes 1179652
  213.4 7.3 %copy-start.25 = (f32[1024]{0:T(1024)S(1)}, f32[1024]{0:T(1024)}, u32[]{:S(2)}) copy-start(f32[1024]{0:T(1024)} %param.26) | copy-start | bytes 12292
  220.3 1.1 copy-start.23
  221.5 3.5 copy-start.18
  224.9 1.2 copy-start.1
  227.1 104.7 %copy-start.22 = (bf16[1,2048,512]{2,1,0:T(8,128)(2,1)S(1)}, bf16[1,2048,512]{2,1,0:T(8,128)(2,1)}, u32[]{:S(2)}) copy-start(bf16[1,2048,512]{2,1,0:T(8,128)(2,1)} %param.31) | copy-start | bytes 6291460
  330.1 1.7 copy-start.3
  343.0 4.5 %copy-start.11 = (s32[192]{0:T(256)S(1)}, s32[192]{0:T(256)}, u32[]{:S(2)}) copy-start(s32[192]{0:T(256)} %copy-done.10) | copy-start | bytes 2308
  343.0 4.5 %copy-start.15 = (s32[192]{0:T(256)S(1)}, s32[192]{0:T(256)}, u32[]{:S(2)}) copy-start(s32[192]{0:T(256)} %copy-done.14) | copy-start | bytes 2308
  343.0 4.7 %copy-start.13 = (s32[192]{0:T(256)S(1)}, s32[192]{0:T(256)}, u32[]{:S(2)}) copy-start(s32[192]{0:T(256)} %copy-done.12) | copy-start | bytes 2308
  343.0 4.7 %copy-start.17 = (s32[192]{0:T(256)S(1)}, s32[192]{0:T(256)}, u32[]{:S(2)}) copy-start(s32[192]{0:T(256)} %copy-done.16) | copy-start | bytes 2308
  343.0 5.0 %copy-start.19 = (f32[192,2]{0,1:T(2,128)S(1)}, f32[192,2]{0,1:T(2,128)}, u32[]{:S(2)}) copy-start(f32[192,2]{0,1:T(2,128)} %param.30) | copy-start | bytes 4612
  343.0 74.3 %all-to-all-start.2 = ((bf16[8,96,2048]{2,1,0:T(8,128)(2,1)}), bf16[8,96,2048]{2,1,0:T(8,128)(2,1)}, u32[]{:S(2)}, u32[]{:S(2)}) async-start(bf16[8,96,2048]{2,1,0:T(8,128)(2,1)} %convolution_convert_fusion), calls=%async_computation.2 | async-start | bytes 6291456 | tf_op jit(solution)/shard_map/all_to_all | solution.py:237
  420.2 1.4 copy-start.2
Sparse Core Ops, SparseCore 0:
  14.3 51.8 all-gather.4
where the time goes:
time: 436 us; the launch traced here: 430 us
  blocking collectives  143 us (33%)
  matrix products  110 us (25%)
  waiting for transfers between devices  76.2 us (17%)
  other arithmetic  35.8 us (8%)
  local copies, waits for them, and re-layouts  27.3 us (6%)
  loops' own time  15.6 us (4%)
  between operations  14 us (3%)
  starting transfers between devices  7.91 us (2%)
    all_to_all x1, blocking collectives, shards(): lax.all_to_all(send_rows, 'sp', split_axis=0, concat_axis=0, tiled=True)  103 us
    all_to_all x1, waiting for transfers between devices, shards(): lax.all_to_all(finished, 'sp', split_axis=0, concat_axis=0, tiled=True)  69.2 us
    unnamed x1, blocking collectives  23.8 us
    dot_general x12, matrix products, block_step(): jnp.dot(keep_weight, k_float, precision=HIGHEST)  18.9 us
    dot_general x12, matrix products, block_step(): jnp.dot(weights_blk, v_block, preferred_element_type=jnp.float32)  18.9 us
    all_gather x1, blocking collectives, prefix(): gathered = jax.tree.map(lambda a: lax.all_gather(a, axis), part)  16.3 us
    another operation x1, loops' own time, block_pass(): lax.scan(block_step, state, (to_blocks(query), to_blocks(keys), to_blocks...  15.6 us
    dot_general x12, matrix products, block_step(): jnp.dot((k_float * keep_weight[:, None]).T, v_block.astype(jnp.float32),...  15.2 us
  transfers between devices with their start and end apart: 3, of which 2 were waited for; matrix products, arithmetic and copies ran while one was open for 31% of the time, Pallas kernels for 0%

commit v1 on v0

v1 whole, which is shorter than its diff:
```python
import functools
import math

import jax
import jax.numpy as jnp
from jax import lax
from jax.experimental import pallas as pl
from jax.experimental.pallas import tpu as pltpu
from jax.sharding import PartitionSpec as P


BLOCK = 64
EPS = 1e-06
FLOOR_LOG = -1e30
AUX_ROWS = 8


def dot(a, b, contract):
    return lax.dot_general(a, b, (contract, ((), ())), preferred_element_type=jnp.float32)


def iota(shape, axis):
    return lax.broadcasted_iota(jnp.int32, shape, axis)


def split_three(x):
    first = x.astype(jnp.bfloat16)
    rest = x - first.astype(jnp.float32)
    second = rest.astype(jnp.bfloat16)
    third = (rest - second.astype(jnp.float32)).astype(jnp.bfloat16)
    return first, second, third


def split_two(x):
    first = x.astype(jnp.bfloat16)
    return first, (x - first.astype(jnp.float32)).astype(jnp.bfloat16)


def pick_rows(rows, count, width):
    row = iota((count, width), 0)
    out = jnp.zeros((count, width), jnp.float32)
    for index, value in enumerate(rows):
        out = jnp.where(row == index, value, out)
    return out


def to_column(row, size):
    eye = iota((size, size), 0) == iota((size, size), 1)
    return jnp.sum(jnp.where(eye, row, 0.0), axis=1, keepdims=True)


def pack_aux(vec, top, total, width):
    return pick_rows([vec, top, total, jnp.ones((1, 1), jnp.float32)], AUX_ROWS, width)


def unpack_aux(aux):
    valid = aux[3:4] > 0.5
    return aux[0:1], jnp.where(valid, aux[1:2], FLOOR_LOG)[:, :1], aux[2:3, :1]


def state_kernel(k_ref, v_ref, forget_ref, input_ref, send_ref, mat_ref, aux_ref, gates_ref, *, chunk):
    seq_len, width = k_ref.shape
    pre = jnp.broadcast_to(forget_ref[...], (8, seq_len))
    log_forget = jnp.minimum(pre, 0.0) - jnp.log1p(jnp.exp(-jnp.abs(pre)))
    cum = jnp.zeros((8, seq_len), jnp.float32)
    upper = (iota((seq_len, seq_len), 0) <= iota((seq_len, seq_len), 1)).astype(jnp.bfloat16)
    for part in reversed(split_three(log_forget)):
        cum = cum + dot(part, upper, ((1,), (0,)))
    level = input_ref[...] - cum
    gates_ref[...] = jnp.where(iota((8, seq_len), 0) == 0, level, cum)
    top = jnp.max(level[:1], axis=1, keepdims=True)
    total = jnp.sum(jnp.where(iota((1, seq_len), 1) == seq_len - 1, cum[:1], 0.0), axis=1, keepdims=True)
    weight = jnp.exp(level[:1] - top)
    mat = jnp.zeros((width, width), jnp.float32)
    vec = jnp.zeros((1, width), jnp.float32)
    for start in range(0, seq_len, chunk):
        here = slice(start, start + chunk)
        column = to_column(weight[:, here], chunk) * width ** (-0.5)
        scaled = k_ref[here, :].astype(jnp.float32) * column
        for part in split_two(scaled):
            vec = vec + jnp.sum(part.astype(jnp.float32), axis=0, keepdims=True)
            mat = mat + dot(part, v_ref[here, :], ((0,), (0,)))
    last = top + total
    mat_ref[...] = mat
    aux_ref[...] = pick_rows([vec, last, total], 8, width)
    send_ref[:width, :] = mat
    send_ref[width:, :] = pack_aux(vec, last, total, width)


def local_kernel(q_ref, k_ref, v_ref, gates_ref, num_ref, stat_ref, *, chunk):
    seq_len, width = q_ref.shape
    key_scale = width ** (-0.5)
    for start in range(0, seq_len, chunk):
        end = start + chunk
        here = slice(start, end)
        scores = dot(q_ref[here, :], k_ref[:end, :], ((1,), (1,))) * key_scale
        row = iota((chunk, end), 0) + start
        col = iota((chunk, end), 1)
        level = jnp.where(col <= row, gates_ref[0:1, :end], -jnp.inf)
        top = jnp.max(level, axis=1, keepdims=True)
        weight = scores * jnp.exp(level - top)
        first = weight.astype(jnp.bfloat16)
        rest = weight - first.astype(jnp.float32)
        own_block = col >= (row // BLOCK) * BLOCK
        second = jnp.where(own_block, 0.0, rest).astype(jnp.bfloat16)
        num_ref[here, :] = dot(first, v_ref[:end, :], ((1,), (0,))) + dot(
            second, v_ref[:end, :], ((1,), (0,))
        )
        den = jnp.sum(first.astype(jnp.float32) + second.astype(jnp.float32), axis=1, keepdims=True)
        cum = to_column(gates_ref[1:2, here], chunk)
        lane = iota((chunk, 128), 1)
        stat_ref[here, :] = jnp.where(lane == 0, den, jnp.where(lane == 1, top, cum))


def merge(old, new):
    old_mat, old_vec, old_max, old_total = old
    new_mat, new_vec, new_max, new_total = new
    joined = jnp.maximum(new_total + old_max, new_max)
    keep_old = jnp.exp(new_total + old_max - joined)
    keep_new = jnp.exp(new_max - joined)
    return (
        keep_old * old_mat + keep_new * new_mat,
        keep_old * old_vec + keep_new * new_vec,
        joined,
        old_total + new_total,
    )


def read_state(mat_ref, aux_ref):
    return (mat_ref[...], aux_ref[0:1, :], aux_ref[1:2, :1], aux_ref[2:3, :1])


def write_state(state, mat_ref, aux_ref):
    mat_ref[...] = state[0]
    aux_ref[...] = pick_rows(state[1:], 8, state[0].shape[1])


def join_kernel(got_ref, mat_ref, aux_ref, far_mat_ref, far_aux_ref, send_ref, mat_out, aux_out, far_mat_out, far_aux_out):
    width = mat_ref.shape[0]
    got = (got_ref[:width, :],) + unpack_aux(got_ref[width:, :])
    state = merge(got, read_state(mat_ref, aux_ref))
    write_state(state, mat_out, aux_out)
    write_state(merge(got, read_state(far_mat_ref, far_aux_ref)), far_mat_out, far_aux_out)
    send_ref[:width, :] = state[0]
    send_ref[width:, :] = pack_aux(*state[1:], width)


def masked(state, valid):
    mat, vec, top, total = state
    return (
        jnp.where(valid, mat, 0.0),
        jnp.where(valid, vec, 0.0),
        jnp.where(valid, top, FLOOR_LOG),
        jnp.where(valid, total, 0.0),
    )


def read_sent(ref):
    width = ref.shape[1]
    return (ref[:width, :],) + unpack_aux(ref[width:, :])


def pair_kernel(place_ref, got_ref, mat_ref, aux_ref, send_ref):
    width = mat_ref.shape[0]
    odd = place_ref[0] % 2 == 1
    own, other = read_state(mat_ref, aux_ref), read_sent(got_ref)
    early = [jnp.where(odd, b, a) for a, b in zip(own, other)]
    late = [jnp.where(odd, a, b) for a, b in zip(own, other)]
    state = merge(early, late)
    send_ref[:width, :] = state[0]
    send_ref[width:, :] = pack_aux(*state[1:], width)


def read_out(far, q_ref, num_ref, stat_ref, out_ref, chunk):
    mat, vec, far_max, _ = far
    mats = split_three(mat)
    for start in range(0, q_ref.shape[0], chunk):
        here = slice(start, start + chunk)
        query = q_ref[here, :]
        den, top, cum = (stat_ref[here, index : index + 1] for index in range(3))
        joined = jnp.maximum(top, far_max)
        keep_own = jnp.exp(top - joined)
        keep_far = jnp.exp(far_max - joined)
        far_num = sum(dot(query, part, ((1,), (0,))) for part in reversed(mats))
        far_den = jnp.sum(query.astype(jnp.float32) * vec, axis=1, keepdims=True)
        num = keep_own * num_ref[here, :] + keep_far * far_num
        den = keep_own * den + keep_far * far_den
        floor = jnp.exp(-(cum + joined))
        out_ref[here, :] = (num / jnp.maximum(jnp.abs(den), floor)).astype(jnp.bfloat16)


def finish_kernel(got_ref, far_mat_ref, far_aux_ref, q_ref, num_ref, stat_ref, out_ref, *, chunk):
    far = merge(read_sent(got_ref), read_state(far_mat_ref, far_aux_ref))
    read_out(far, q_ref, num_ref, stat_ref, out_ref, chunk)


def finish_pairs_kernel(place_ref, *refs, chunk, far_count):
    place = place_ref[0]
    width = refs[0].shape[1]
    far = (jnp.zeros((width, width), jnp.float32), jnp.zeros((1, width), jnp.float32))
    far += (jnp.full((1, 1), FLOOR_LOG, jnp.float32), jnp.zeros((1, 1), jnp.float32))
    for back in range(far_count, 0, -1):
        far = merge(far, masked(read_sent(refs[back]), place // 2 >= back))
    far = merge(far, masked(read_sent(refs[0]), place % 2 == 1))
    read_out(far, *refs[far_count + 1 :], chunk)


def call(kernel, outs, *args, specs=None, scratch=(), vmem=16, flops=0, **kwargs):
    extra = {} if specs is None else {"in_specs": specs}
    if flops:
        extra["cost_estimate"] = pl.CostEstimate(flops=flops, transcendentals=0, bytes_accessed=0)
    return pl.pallas_call(
        functools.partial(kernel, **kwargs),
        out_shape=[jax.ShapeDtypeStruct(shape, dtype) for shape, dtype in outs],
        scratch_shapes=scratch,
        compiler_params=pltpu.CompilerParams(vmem_limit_bytes=vmem * 2**20),
        **extra,
    )(*args)


SCALAR = pl.BlockSpec(memory_space=pltpu.SMEM)
VECTOR = pl.BlockSpec(memory_space=pltpu.VMEM)
REMOTE = pl.BlockSpec(memory_space=pltpu.HBM)
RING = 4
VMEM_SLOT = 36


def ring_shift(array, step=1):
    places = lax.axis_size("sp")
    return lax.ppermute(array, "sp", [(place, (place + 2 * step) % places) for place in range(places)])


def pair_swap(array):
    return lax.ppermute(array, "sp", [(place, place ^ 1) for place in range(lax.axis_size("sp"))])


def side_swap(array, distance):
    return lax.ppermute(array, "tp", [(place, place ^ distance) for place in range(lax.axis_size("tp"))])


def ring_fits():
    places = lax.axis_size("sp")
    return places == 2 * RING and lax.axis_size("tp") % 4 == 0


def cell_head(query, keys, values, forget_pre, input_pre):
    seq_len, width = query.shape
    chunk = math.gcd(seq_len, 128)
    f32, b16 = jnp.float32, jnp.bfloat16
    states = [((width, width), f32), ((8, width), f32)]
    sent = [((width + AUX_ROWS, width), f32)]
    send, mat, aux, gates = call(
        state_kernel,
        sent + states + [((8, seq_len), f32)],
        keys,
        values,
        forget_pre,
        input_pre,
        vmem=56,
        chunk=chunk,
    )
    num, stat = call(
        local_kernel, [((seq_len, width), f32), ((seq_len, 128), f32)], query, keys, values, gates, chunk=chunk
    )
    if ring_fits():
        place = lax.axis_index("sp").astype(jnp.int32).reshape(1)
        pair = pair_swap(send)
        slab = call(pair_kernel, sent, place, pair, mat, aux, specs=[SCALAR] + [VECTOR] * 3)[0]
        far_count = lax.axis_size("sp") // 2 - 1
        fars = []
        for back in range(far_count):
            fars.append(ring_shift(slab, back + 1))
        operands = [pair, *fars, query, num, stat]
        rows = call(
            finish_pairs_kernel,
            [((seq_len, width), b16)],
            place,
            *operands,
            specs=[SCALAR] + [VECTOR] * len(operands),
            chunk=chunk,
            far_count=far_count,
        )[0]
        return rows, (send, stat, fars, rows)
    far_mat = jnp.zeros((width, width), f32)
    far_aux = jnp.where(iota((8, width), 0) == 1, FLOOR_LOG, 0.0)
    places = lax.axis_size("sp")
    step = 1
    got = jnp.zeros(sent[0][0], f32)
    while step < places:
        got = lax.ppermute(send, "sp", [(place, place + step) for place in range(places - step)])
        step *= 2
        if step < places:
            send, mat, aux, far_mat, far_aux = call(
                join_kernel, sent + states + states, got, mat, aux, far_mat, far_aux
            )
    rows = call(
        finish_kernel, [((seq_len, width), b16)], got, far_mat, far_aux, query, num, stat, chunk=chunk
    )[0]
    return rows, got


def mix_kernel(rows_ref, gate_ref, gain_ref, proj_ref, resid_ref, ffn_gain_ref, mix_ref, norm_ref):
    rows = rows_ref[...].astype(jnp.float32)
    headed = rows * lax.rsqrt(jnp.mean(rows * rows, axis=1, keepdims=True) + EPS) * gain_ref[...]
    gated = (headed * jax.nn.sigmoid(gate_ref[...].astype(jnp.float32))).astype(jnp.bfloat16)
    mix = resid_ref[...].astype(jnp.float32) + dot(gated, proj_ref[...], ((1,), (0,)))
    mix_ref[...] = mix
    norm = mix * lax.rsqrt(jnp.mean(mix * mix, axis=1, keepdims=True) + EPS) * ffn_gain_ref[...]
    norm_ref[...] = norm.astype(jnp.bfloat16)


def gate_kernel(heads_ref, gate_ref, gain_ref, out_ref):
    count, _, width = heads_ref.shape
    heads = [heads_ref[head].astype(jnp.float32) for head in range(count)]
    squares = sum(jnp.sum(rows * rows, axis=1, keepdims=True) for rows in heads)
    scale = lax.rsqrt(squares / (count * width) + EPS)
    for head, rows in enumerate(heads):
        here = slice(head * width, (head + 1) * width)
        gate = jax.nn.sigmoid(gate_ref[:, here].astype(jnp.float32))
        out_ref[:, here] = (rows * scale * gain_ref[:, here] * gate).astype(jnp.bfloat16)


def route_kernel(routes_ref, scores_ref, out_ref, *, expert_count):
    scores = scores_ref[...]
    weight = scores / jnp.sum(scores, axis=0, keepdims=True)
    row = iota(out_ref.shape, 0)
    dense = jnp.zeros(out_ref.shape, jnp.float32)
    for route in range(scores.shape[0]):
        named = row % expert_count == routes_ref[route : route + 1, :]
        dense = dense + jnp.where(named, weight[route : route + 1, :], 0.0)
    first, second, third = (part.astype(jnp.float32) for part in split_three(dense))
    place = row // expert_count
    packed = jnp.where(place == 0, first, jnp.where(place == 1, second, third))
    out_ref[...] = jnp.where(place < 3, packed, 0.0).astype(jnp.bfloat16)


def expert_weight(route_ref, expert_count, expert):
    row = iota(route_ref.shape, 0)
    mine = (row % expert_count == expert) & (row < 3 * expert_count)
    weight = jnp.sum(jnp.where(mine, route_ref[...].astype(jnp.float32), 0.0), axis=0, keepdims=True)
    return to_column(weight, route_ref.shape[1])


def mix_rows(gated_ref, resid_ref, proj, gain_ref):
    mix = resid_ref[...].astype(jnp.float32) + dot(gated_ref[...], proj, ((1,), (0,)))
    norm = mix * lax.rsqrt(jnp.mean(mix * mix, axis=1, keepdims=True) + EPS) * gain_ref[...]
    return mix, norm.astype(jnp.bfloat16)


def own_mix_kernel(gated_ref, resid_ref, gain_ref, proj_ref, mix_ref, norm_ref):
    mix_ref[...], norm_ref[...] = mix_rows(gated_ref, resid_ref, proj_ref[...], gain_ref)


def slot_kernel(place_ref, route_ref, *refs, expert_count, given, count):
    lead, sources, out_ref = refs[:given], refs[given : given + count], refs[given + count]
    places, sems = refs[given + count + 1 : -1], refs[-1]
    solid = count - 12
    targets = list(places[:solid])
    _, part = sources[solid].shape
    for index in range(4):
        here = pl.ds(index * part, part)
        targets += [
            places[solid].at[:, here],
            places[solid + 1].at[:, here],
            places[solid + 2].at[here, :],
        ]
    copies = [
        pltpu.make_async_copy(source, target, sems.at[index])
        for index, (source, target) in enumerate(zip(sources, targets))
    ]
    order = list(range(solid))
    order += [solid + 3 * quarter + kind for kind in range(3) for quarter in range(4)]
    for index in order:
        copies[index].start()

    def ready(place):
        for index in [place] if place < solid else range(place, count, 3):
            copies[index].wait()
        return places[place][...]

    if solid == 4:
        gated_ref, resid_ref, gain_ref = lead
        _, rows = mix_rows(gated_ref, resid_ref, ready(0), gain_ref)
    else:
        rows = lead[0][...]

    def expert_part(first):
        gate = dot(rows, ready(first), ((1,), (0,)))
        up = dot(rows, ready(first + 1), ((1,), (0,)))
        active = (jax.nn.silu(gate) * up).astype(jnp.bfloat16)
        return dot(active, ready(first + 2), ((1,), (0,))).astype(jnp.bfloat16).astype(jnp.float32)

    place = place_ref[0]
    other = place + 1 - 2 * (place % 2)
    total = expert_part(solid - 3) * expert_weight(route_ref, expert_count, place)
    total = total + expert_part(solid) * expert_weight(route_ref, expert_count, other)
    if given == 2:
        total = total + lead[1][...]
    out_ref[...] = total.astype(out_ref.dtype)


def part_size(arrays):
    return sum(math.prod(array.shape) for array in arrays)


def ring_experts(lead_in, cell_parts, gated, ffn_gain, out_proj, w_gate, w_up, w_down):
    resid, routes, route_scores = lead_in
    places = lax.axis_size("sp")
    rows, width = resid.shape
    place = lax.axis_index("sp").astype(jnp.int32).reshape(1)
    names = -(-3 * places // 16) * 16
    routed = call(
        route_kernel, [((names, rows), jnp.bfloat16)], routes.T, route_scores.T, expert_count=places
    )[0]
    send, stat, fars, cell_rows = cell_parts
    part = w_gate.shape[2] // 4
    quarter = lax.axis_index("tp") % 4
    quarters = [
        lax.dynamic_slice_in_dim(w_gate[0], quarter * part, part, 1),
        lax.dynamic_slice_in_dim(w_up[0], quarter * part, part, 1),
        lax.dynamic_slice_in_dim(w_down[0], quarter * part, part, 0),
        lax.dynamic_slice_in_dim(w_down[0], (quarter ^ 2) * part, part, 0),
    ]
    quarters, _ = lax.optimization_barrier((quarters, send))
    near, cross, far = [], [], []
    for index in range(4):
        near.append(pair_swap(quarters[index]))
    for index, token in enumerate((stat, cell_rows)):
        source, _ = lax.optimization_barrier((near[index], token))
        cross.append(side_swap(source, 2))
    cross.append(near.pop())
    for quarter in near + cross:
        source, _ = lax.optimization_barrier((quarter, gated))
        far.append(side_swap(source, 1))
    parts = [*near, *cross, *far]
    experts = [w_gate[0], w_up[0], w_down[0]]

    def slot(shared, lead, dtype):
        solid = ([out_proj] if len(lead) == 3 else []) + experts
        weights = solid + parts
        return call(
            slot_kernel,
            [((rows, width), dtype)],
            place,
            shared,
            *lead,
            *weights,
            specs=[SCALAR] + [VECTOR] * (1 + len(lead)) + [REMOTE] * len(weights),
            scratch=[pltpu.VMEM(array.shape, array.dtype) for array in solid + experts]
            + [pltpu.SemaphoreType.DMA((len(weights),))],
            vmem=VMEM_SLOT,
            flops=2 * rows * part_size(weights),
            expert_count=places,
            given=len(lead),
            count=len(weights),
        )[0]

    routed_late, _ = lax.optimization_barrier((routed, stat))
    shares = [routed]
    for back in range(1, RING):
        shares.append(ring_shift(routed_late, back))
    gain = ffn_gain[None, :]
    lead_one = ring_shift(resid)
    lead_two = ring_shift(lax.optimization_barrier((lead_one, *fars))[0])
    gated_one = ring_shift(gated)
    gated_two = ring_shift(gated_one)
    mix, norm = call(
        own_mix_kernel,
        [((rows, width), jnp.float32), ((rows, width), jnp.bfloat16)],
        gated,
        resid,
        gain,
        out_proj,
        flops=2 * rows * out_proj.size,
    )
    norm_next = ring_shift(norm, -1)
    b16, f32 = jnp.bfloat16, jnp.float32
    part_two = slot(shares[2], (gated_two, lead_two, gain), b16)
    sum_two = ring_shift(part_two)
    part_one = slot(shares[1], (gated_one, lead_one, gain), b16)
    sum_one = ring_shift(part_one, -1)
    part_next = slot(shares[3], (norm_next,), b16)
    sum_next = ring_shift((part_next.astype(f32) + sum_two.astype(f32)).astype(b16))
    total = slot(routed, (norm, mix), f32)
    total = total + sum_one.astype(f32) + sum_next.astype(f32)
    return total.astype(jnp.bfloat16)


def slot_select(expert_ids, expert_count, capacity):
    flat_ids = expert_ids.reshape(-1)
    one_hot = (flat_ids[:, None] == jnp.arange(expert_count, dtype=jnp.int32)[None, :]).astype(
        jnp.int32
    )
    slot_rank = jnp.sum((jnp.cumsum(one_hot, axis=0) - 1) * one_hot, axis=1)
    target = flat_ids * capacity + slot_rank
    return (
        jnp.arange(expert_count * capacity, dtype=jnp.int32)[:, None] == target[None, :]
    ).astype(jnp.bfloat16)


def run_experts(arrived, w_gate, w_up, w_down, sources):
    local_count = w_gate.shape[0]
    grouped = arrived.reshape(sources, local_count, arrived.shape[1], arrived.shape[2])
    gate_pre = jnp.einsum("pesd,edf->pesf", grouped, w_gate, preferred_element_type=jnp.float32)
    up_pre = jnp.einsum("pesd,edf->pesf", grouped, w_up, preferred_element_type=jnp.float32)
    active = (jax.nn.silu(gate_pre) * up_pre).astype(jnp.bfloat16)
    result = jnp.einsum(
        "pesf,efd->pesd", active, w_down, preferred_element_type=jnp.float32
    ).astype(jnp.bfloat16)
    return result.reshape(arrived.shape)


def shards(
    resid,
    query,
    keys,
    values,
    out_gate,
    forget_pre,
    input_pre,
    head_gain,
    out_proj,
    ffn_gain,
    routes,
    route_scores,
    w_gate,
    w_up,
    w_down,
):
    local_heads = forget_pre.shape[0]
    seq_len = query.shape[0]
    head_width = query.shape[1] // local_heads
    heads = [
        cell_head(
            query[:, head * head_width : (head + 1) * head_width],
            keys[:, head * head_width : (head + 1) * head_width],
            values[:, head * head_width : (head + 1) * head_width],
            forget_pre[head : head + 1],
            input_pre[head : head + 1],
        )
        for head in range(local_heads)
    ]
    cell_parts = heads[0][1]
    cell_rows = jnp.concatenate([head[0] for head in heads], axis=1)
    if ring_fits() and w_gate.shape[0] == 1 and local_heads == 1 and w_gate.shape[2] % 512 == 0:
        tokens = seq_len // lax.axis_size("tp")
        token_heads = lax.all_to_all(
            cell_rows.reshape(-1, tokens, head_width), "tp", split_axis=0, concat_axis=0, tiled=True
        )
        gated = call(
            gate_kernel,
            [((tokens, out_gate.shape[1]), jnp.bfloat16)],
            token_heads,
            out_gate,
            head_gain[None, :],
        )[0]
        lead_in = (resid, routes, route_scores)
        return ring_experts(lead_in, cell_parts, gated, ffn_gain, out_proj, w_gate, w_up, w_down)
    token_rows = lax.all_to_all(cell_rows, "tp", split_axis=0, concat_axis=1, tiled=True)
    wide = resid.shape
    after_mix, normed_rows = call(
        mix_kernel,
        [(wide, jnp.float32), (wide, jnp.bfloat16)],
        token_rows,
        out_gate,
        head_gain[None, :],
        out_proj,
        resid,
        ffn_gain[None, :],
    )
    row_count = normed_rows.shape[0]
    half_rows = row_count // 2
    route_count = routes.shape[1]
    sources = lax.axis_size("sp")
    expert_count = w_gate.shape[0] * sources
    capacity = max(2, 2 * half_rows * route_count // expert_count)
    selects = [
        slot_select(
            routes[half_idx * half_rows : (half_idx + 1) * half_rows], expert_count, capacity
        )
        for half_idx in range(2)
    ]

    def pack_rows(half_idx):
        selection = (
            selects[half_idx].reshape(expert_count * capacity, half_rows, route_count).sum(axis=2)
        )
        packed = jnp.dot(
            selection,
            normed_rows[half_idx * half_rows : (half_idx + 1) * half_rows],
            preferred_element_type=jnp.float32,
        )
        return packed.astype(jnp.bfloat16).reshape(expert_count, capacity, normed_rows.shape[1])

    send_rows = jnp.concatenate([pack_rows(0), pack_rows(1)], axis=1)
    finished = run_experts(
        lax.all_to_all(send_rows, "sp", split_axis=0, concat_axis=0, tiled=True),
        w_gate,
        w_up,
        w_down,
        sources,
    )
    returned = lax.all_to_all(finished, "sp", split_axis=0, concat_axis=0, tiled=True)
    answers = [returned[:, :capacity], returned[:, capacity:]]
    route_weight = route_scores / jnp.sum(route_scores, axis=1, keepdims=True)
    pieces = []
    for half_idx in range(2):
        gathered = lax.dot_general(
            selects[half_idx],
            answers[half_idx].reshape(expert_count * capacity, -1),
            (((0,), (0,)), ((), ())),
            preferred_element_type=jnp.float32,
        )
        weights_half = route_weight[half_idx * half_rows : (half_idx + 1) * half_rows]
        pieces.append(
            jnp.sum(gathered.reshape(half_rows, route_count, -1) * weights_half[:, :, None], axis=1)
        )
    return (after_mix + jnp.concatenate(pieces, axis=0)).astype(jnp.bfloat16)


def solution(mesh):
    placed = (
        P(("sp", "tp"), None),
        P("sp", "tp"),
        P("sp", "tp"),
        P("sp", "tp"),
        P(("sp", "tp"), None),
        P("tp", "sp"),
        P("tp", "sp"),
        P(),
        P(),
        P(),
        P(("sp", "tp"), None),
        P(("sp", "tp"), None),
        P("sp", None, None),
        P("sp", None, None),
        P("sp", None, None),
    )
    return jax.shard_map(
        shards, mesh=mesh, in_specs=placed, out_specs=P(("sp", "tp"), None), check_vma=False
    )
```

time: 436 us -> 216 us (0.50); the launches traced: 430 us -> 216 us
  blocking collectives: 143 us -> 0 us
  matrix products: 110 us -> 0 us
  waiting for transfers between devices: 76.2 us -> 130 us
  other arithmetic: 35.8 us -> 1.5 us
  Pallas kernels: 0 us -> 33.3 us
  starting transfers between devices: 7.91 us -> 34.4 us
  loops' own time: 15.6 us -> 0 us
  between operations: 14 us -> 0.29 us
  local copies, waits for them, and re-layouts: 27.3 us -> 16.5 us
    ppermute x0 -> x27, waiting for transfers between devices: none -> 130 us  [the longest x14 104 us: ring_shift(): lax.ppermute(array, 'sp', [(place, (place + 2 * step) % places) for place...]
    dot_general x83 -> x0, matrix products: 110 us -> none  [the longest x12 18.9 us: block_step(): jnp.dot(keep_weight, k_float, precision=HIGHEST)]
    all_to_all x1 -> x0, blocking collectives: 103 us -> none  [shards(): lax.all_to_all(send_rows, 'sp', split_axis=0, concat_axis=0, tiled=True)]
    all_to_all x2 -> x1, waiting for transfers between devices: 76.1 us -> 0.01 us  [shards(): lax.all_to_all(cell_rows.reshape(-1, tokens, head_width), 'tp', split_axi...]
    pallas_call x0 -> x11, Pallas kernels: none -> 33.3 us  [call(): pl.pallas_call(functools.partial(kernel, **kwargs), out_shape=[jax.ShapeD...]
    ppermute x0 -> x27, starting transfers between devices: none -> 30.8 us  [the longest x14 17.8 us: ring_shift(): lax.ppermute(array, 'sp', [(place, (place + 2 * step) % places) for place...]
    unnamed x1 -> x0, blocking collectives: 23.8 us -> none
    reduce_max x25 -> x0, other arithmetic: 17.8 us -> none  [the longest x12 14.6 us: block_step(): new_max = jnp.maximum(block_total + max_log, jnp.max(log_keep))]
  transfers between devices with their start and end apart: 3 -> 28, of which waited for: 2 -> 11; matrix products, arithmetic and copies ran while one was open for 31% -> 0% of each run, Pallas kernels for 0% -> 14%
where the time goes in v1:
time: 216 us
  waiting for transfers between devices  130 us (60%)
  starting transfers between devices  34.4 us (16%)
  Pallas kernels  33.3 us (15%)
  local copies, waits for them, and re-layouts  16.5 us (8%)
    ppermute x14, waiting for transfers between devices, ring_shift(): lax.ppermute(array, 'sp', [(place, (place + 2 * step) % places) for place...  104 us
    pallas_call x11, Pallas kernels, call(): pl.pallas_call(functools.partial(kernel, **kwargs), out_shape=[jax.ShapeD...  33.3 us
    ppermute x14, starting transfers between devices, ring_shift(): lax.ppermute(array, 'sp', [(place, (place + 2 * step) % places) for place...  17.8 us
    ppermute x5, waiting for transfers between devices, pair_swap(): lax.ppermute(array, 'sp', [(place, place ^ 1) for place in range(lax.axis...  16.9 us
    unnamed x44, local copies, waits for them, and re-layouts  11.9 us
    ppermute x8, waiting for transfers between devices, side_swap(): lax.ppermute(array, 'tp', [(place, place ^ distance) for place in range(l...  9.13 us
    ppermute x5, starting transfers between devices, pair_swap(): lax.ppermute(array, 'sp', [(place, place ^ 1) for place in range(lax.axis...  8.07 us
    ppermute x8, starting transfers between devices, side_swap(): lax.ppermute(array, 'tp', [(place, place ^ distance) for place in range(l...  4.85 us
  transfers between devices with their start and end apart: 28, of which 11 were waited for; matrix products, arithmetic and copies ran while one was open for 0% of the time, Pallas kernels for 14%

profile of v1, /device:TPU:0, one launch (start us, length us, event | category | flops | bytes accessed | tf_op | source)
XLA Modules:
  0.0 215.5 jit_solution(7547582121583852736)
XLA Ops:
  0.0 2.4 %dynamic-slice_bitcast_fusion = (bf16[128,2048]{1,0:T(8,128)(2,1)}, bf16[128,2048]{1,0:T(8,128)(2,1)}) fusion(bf16[1,512,2048]{2,1,0:T(8,128)(2,1)} %param.29, s32[]{:T(128)S(6)} %select_n.17, s32[]{:T(128)S(6)} %select_n.16), kind=kLoop, calls=%fused_computation.2 | loop fusion | bytes 2097160 | tf_op jit(solution)/shard_map/dynamic_slice | solution.py:422
  2.4 2.1 dynamic-slice_bitcast_fusion.2
  4.6 3.4 %shard_map.146 = (f32[264,256]{1,0:T(8,128)}, f32[256,256]{1,0:T(8,128)}, f32[8,256]{1,0:T(8,128)}, f32[8,768]{1,0:T(8,128)}) custom-call(bf16[768,256]{1,0:T(8,128)(2,1)} %k_ref.3, bf16[768,256]{1,0:T(8,128)(2,1)} %v_ref.3, f32[1,768]{1,0:T(1,128)} %forget_ref.1, f32[1,768]{1,0:T(1,128)} %input_ref.1), custom_call_target="tpu_custom_call" | custom-call | tf_op jit(solution)/shard_map/pallas_call | solution.py:212
  8.0 3.0 %collective-permute-start.4 = (bf16[2048,128]{1,0:T(8,128)(2,1)}, bf16[2048,128]{1,0:T(8,128)(2,1)S(1)}, u32[]{:S(2)}, u32[]{:S(2)}) collective-permute-start(bf16[2048,128]{1,0:T(8,128)(2,1)} %get-tuple-element.35), channel_id=1, source_target_pairs={{0,4},{4,0},{8,12},{12,8},{16,20},{20,16},{24,28},{28,24},{1,5},{5... | collective-permute-start | bytes 1572872 | tf_op jit(solution)/shard_map/ppermute | solution.py:234
  11.0 2.0 collective-permute-start.5
  13.0 16.9 %collective-permute-done.got_ref.refs_0_ = f32[264,256]{1,0:T(8,128)} collective-permute-done((f32[264,256]{1,0:T(8,128)}, f32[264,256]{1,0:T(8,128)}, u32[]{:S(2)}, u32[]{:S(2)}) %collective-permute-start) | collective-permute-done | bytes 270368 | tf_op jit(solution)/shard_map/ppermute | solution.py:234
  32.6 4.2 %collective-permute-start.3 = (f32[264,256]{1,0:T(8,128)S(1)}, f32[264,256]{1,0:T(8,128)S(1)}, u32[]{:S(2)}, u32[]{:S(2)}) collective-permute-start(f32[264,256]{1,0:T(8,128)S(1)} %shard_map.147), channel_id=1, source_target_pairs={{0,24},{4,28},{8,0},{12,4},{16,8},{20,12},{24,16},{28,20},{1,25},{... | collective-permute-start | bytes 811016 | tf_op jit(solution)/shard_map/ppermute | solution.py:230
  37.8 2.5 %collective-permute-start.18 = (bf16[192,2048]{1,0:T(8,128)(2,1)}, bf16[192,2048]{1,0:T(8,128)(2,1)}, u32[]{:S(2)}, u32[]{:S(2)}) collective-permute-start(bf16[192,2048]{1,0:T(8,128)(2,1)} %resid_ref.1), channel_id=1, source_target_pairs={{0,8},{4,12},{8,16},{12,20},{16,24},{20,28},{24,0},{28,4},{1,9},{5... | collective-permute-start | bytes 2359304 | tf_op jit(solution)/shard_map/ppermute | solution.py:230
  40.3 3.4 %collective-permute-done.3.refs_3_ = f32[264,256]{1,0:T(8,128)S(1)} collective-permute-done((f32[264,256]{1,0:T(8,128)S(1)}, f32[264,256]{1,0:T(8,128)S(1)}, u32[]{:S(2)}, u32[]{:S(2)}) %collective-permute-start.3) | collective-permute-done | bytes 270368 | tf_op jit(solution)/shard_map/ppermute | solution.py:230
  45.2 29.7 %collective-permute-done.2.refs_2_ = f32[264,256]{1,0:T(8,128)S(1)} collective-permute-done((f32[264,256]{1,0:T(8,128)S(1)}, f32[264,256]{1,0:T(8,128)S(1)}, u32[]{:S(2)}, u32[]{:S(2)}) %collective-permute-start.2) | collective-permute-done | bytes 270368 | tf_op jit(solution)/shard_map/ppermute | solution.py:230
  79.1 1.5 shard_map.148
  80.7 1.6 collective-permute-start.7
  82.3 2.7 %shard_map.149 = bf16[768,256]{1,0:T(8,128)(2,1)S(1)} custom-call(s32[1]{0:T(128)} %bitcast.place_ref, f32[264,256]{1,0:T(8,128)} %collective-permute-done.got_ref.refs_0_, f32[264,256]{1,0:T(8,128)S(1)} %collective-permute-done.1.refs_1_, f32[264,256]{1,0:T(8,128)S(1)} %collective-permute-done.2.refs_2_, f32[264,256]{1,0:T(8,128)S(1)} %collective-permute-done.3.refs_3_, ...), custom_call_target="tpu_custom_call" | custom-call | tf_op jit(solution)/shard_map/pallas_call | solution.py:212
  85.7 3.6 %all-to-all-start = ((bf16[4,192,256]{2,1,0:T(8,128)(2,1)}), bf16[4,192,256]{2,1,0:T(8,128)(2,1)S(1)}, u32[]{:S(2)}, u32[]{:S(2)}) async-start(bf16[4,192,256]{2,1,0:T(8,128)(2,1)} %bitcast.29), calls=%async_computation | async-start | bytes 786432 | tf_op jit(solution)/shard_map/all_to_all | solution.py:547
  90.2 4.6 %collective-permute-done.22.route_ref = bf16[32,192]{1,0:T(8,128)(2,1)S(1)} collective-permute-done((bf16[32,192]{1,0:T(8,128)(2,1)S(1)}, bf16[32,192]{1,0:T(8,128)(2,1)S(1)}, u32[]{:S(2)}, u32[]{:S(2)}) %collective-permute-start.22) | collective-permute-done | bytes 12320 | tf_op jit(solution)/shard_map/ppermute | solution.py:230
  95.4 2.0 collective-permute-start.8
  99.5 9.1 %collective-permute-done.8.refs_9_.refs_11_.refs_8_ = bf16[2048,128]{1,0:T(8,128)(2,1)} collective-permute-done((bf16[2048,128]{1,0:T(8,128)(2,1)S(1)}, bf16[2048,128]{1,0:T(8,128)(2,1)}, u32[]{:S(2)}, u32[]{:S(2)}) %collective-permute-start.8) | collective-permute-done | bytes 524320 | tf_op jit(solution)/shard_map/ppermute | solution.py:238
  108.6 4.2 %collective-permute-done.17.refs_0_ = bf16[192,1024]{1,0:T(8,128)(2,1)S(1)} collective-permute-done((bf16[192,1024]{1,0:T(8,128)(2,1)S(1)}, bf16[192,1024]{1,0:T(8,128)(2,1)S(1)}, u32[]{:S(2)}, u32[]{:S(2)}) %collective-permute-start.17) | collective-permute-done | bytes 393248 | tf_op jit(solution)/shard_map/ppermute | solution.py:230
  113.5 2.2 %copy-done.3 = bf16[1024,2048]{1,0:T(8,128)(2,1)S(1)} copy-done((bf16[1024,2048]{1,0:T(8,128)(2,1)S(1)}, bf16[1024,2048]{1,0:T(8,128)(2,1)}, u32[]{:S(2)}) %copy-start.3) | copy-done | bytes 4194328
  116.8 3.9 %collective-permute-start.21 = (bf16[192,2048]{1,0:T(8,128)(2,1)S(1)}, bf16[192,2048]{1,0:T(8,128)(2,1)S(1)}, u32[]{:S(2)}, u32[]{:S(2)}) collective-permute-start(bf16[192,2048]{1,0:T(8,128)(2,1)S(1)} %get-tuple-element.33.refs_0_), channel_id=1, source_target_pairs={{0,24},{4,28},{8,0},{12,4},{16,8},{20,12},{24,16},{28,20},{1,25},{... | collective-permute-start | bytes 2359304 | tf_op jit(solution)/shard_map/ppermute | solution.py:230
  120.7 10.5 %collective-permute-done.24.refs_1_ = bf16[192,2048]{1,0:T(8,128)(2,1)S(1)} collective-permute-done((bf16[192,2048]{1,0:T(8,128)(2,1)}, bf16[192,2048]{1,0:T(8,128)(2,1)S(1)}, u32[]{:S(2)}, u32[]{:S(2)}) %collective-permute-start.24) | collective-permute-done | bytes 786464 | tf_op jit(solution)/shard_map/ppermute | solution.py:230
  131.3 8.3 %collective-permute-done.23.refs_0_ = bf16[192,1024]{1,0:T(8,128)(2,1)S(1)} collective-permute-done((bf16[192,1024]{1,0:T(8,128)(2,1)S(1)}, bf16[192,1024]{1,0:T(8,128)(2,1)S(1)}, u32[]{:S(2)}, u32[]{:S(2)}) %collective-permute-start.23) | collective-permute-done | bytes 393248 | tf_op jit(solution)/shard_map/ppermute | solution.py:230
  139.6 2.2 %copy-done.4 = bf16[1024,2048]{1,0:T(8,128)(2,1)S(1)} copy-done((bf16[1024,2048]{1,0:T(8,128)(2,1)S(1)}, bf16[1024,2048]{1,0:T(8,128)(2,1)}, u32[]{:S(2)}) %copy-start.4) | copy-done | bytes 4194328
  141.8 6.2 %shard_map.155 = bf16[192,2048]{1,0:T(8,128)(2,1)S(1)} custom-call(s32[1]{0:T(128)} %bitcast.place_ref, bf16[32,192]{1,0:T(8,128)(2,1)S(1)} %copy-done.17, bf16[192,1024]{1,0:T(8,128)(2,1)S(1)} %collective-permute-done.23.refs_0_, bf16[192,2048]{1,0:T(8,128)(2,1)S(1)} %collective-permute-done.24.refs_1_, f32[1,2048]{1,0:T(1,128)S(1)} %bitcast.31, ...), custom_call_target="tpu_custom_call" | custom-call | flops 3221225472 | tf_op jit(solution)/shard_map/pallas_call | solution.py:212
  148.3 3.8 %collective-permute-start.20 = (bf16[32,192]{1,0:T(8,128)(2,1)S(1)}, bf16[32,192]{1,0:T(8,128)(2,1)S(1)}, u32[]{:S(2)}, u32[]{:S(2)}) collective-permute-start(bf16[32,192]{1,0:T(8,128)(2,1)S(1)} %copy-done.14), channel_id=1, source_target_pairs={{0,24},{4,28},{8,0},{12,4},{16,8},{20,12},{24,16},{28,20},{1,25},{... | collective-permute-start | bytes 36872 | tf_op jit(solution)/shard_map/ppermute | solution.py:230
  152.1 19.8 %collective-permute-done.16.route_ref = bf16[32,192]{1,0:T(8,128)(2,1)S(1)} collective-permute-done((bf16[32,192]{1,0:T(8,128)(2,1)S(1)}, bf16[32,192]{1,0:T(8,128)(2,1)S(1)}, u32[]{:S(2)}, u32[]{:S(2)}) %collective-permute-start.16) | collective-permute-done | bytes 12320 | tf_op jit(solution)/shard_map/ppermute | solution.py:230
  171.9 7.3 %shard_map.153 = bf16[192,2048]{1,0:T(8,128)(2,1)S(1)} custom-call(s32[1]{0:T(128)} %bitcast.place_ref, bf16[32,192]{1,0:T(8,128)(2,1)S(1)} %collective-permute-done.16.route_ref, bf16[192,1024]{1,0:T(8,128)(2,1)S(1)} %collective-permute-done.17.refs_0_, bf16[192,2048]{1,0:T(8,128)(2,1)} %collective-permute-done.18.refs_1_, f32[1,2048]{1,0:T(1,128)S(1)} %bitcast.32, ...), custom_call_target="tpu_custom_call" | custom-call | flops 3221225472 | tf_op jit(solution)/shard_map/pallas_call | solution.py:212
  179.5 4.7 %shard_map.154 = bf16[192,2048]{1,0:T(8,128)(2,1)S(1)} custom-call(s32[1]{0:T(128)} %bitcast.place_ref, bf16[32,192]{1,0:T(8,128)(2,1)S(1)} %collective-permute-done.20.route_ref, bf16[192,2048]{1,0:T(8,128)(2,1)S(1)} %collective-permute-done.21.refs_0_, bf16[2048,512]{1,0:T(8,128)(2,1)S(1)} %bitcast.23, bf16[2048,512]{1,0:T(8,128)(2,1)S(1)} %bitcast.27, ...), custom_call_target="tpu_custom_call" | custom-call | flops 2415919104 | tf_op jit(solution)/shard_map/pallas_call | solution.py:212
  184.6 1.9 collective-permute-start.26
  186.4 4.8 %shard_map.152 = f32[192,2048]{1,0:T(8,128)S(1)} custom-call(s32[1]{0:T(128)} %bitcast.place_ref, bf16[32,192]{1,0:T(8,128)(2,1)S(1)} %copy-done.14, bf16[192,2048]{1,0:T(8,128)(2,1)S(1)} %get-tuple-element.33.refs_0_, f32[192,2048]{1,0:T(8,128)S(1)} %get-tuple-element.34.refs_1_, bf16[2048,512]{1,0:T(8,128)(2,1)S(1)} %bitcast.24, ...), custom_call_target="tpu_custom_call" | custom-call | flops 2415919104 | tf_op jit(solution)/shard_map/pallas_call | solution.py:212
  191.2 6.3 %collective-permute-done.19 = bf16[192,2048]{1,0:T(8,128)(2,1)S(1)} collective-permute-done((bf16[192,2048]{1,0:T(8,128)(2,1)S(1)}, bf16[192,2048]{1,0:T(8,128)(2,1)S(1)}, u32[]{:S(2)}, u32[]{:S(2)}) %collective-permute-start.19) | collective-permute-done | bytes 786464 | tf_op jit(solution)/shard_map/ppermute | solution.py:230
  197.5 16.8 %collective-permute-done.26 = bf16[192,2048]{1,0:T(8,128)(2,1)S(1)} collective-permute-done((bf16[192,2048]{1,0:T(8,128)(2,1)S(1)}, bf16[192,2048]{1,0:T(8,128)(2,1)S(1)}, u32[]{:S(2)}, u32[]{:S(2)}) %collective-permute-start.26) | collective-permute-done | bytes 786464 | tf_op jit(solution)/shard_map/ppermute | solution.py:230
  (83 shorter events, 17.8 us)
Async XLA Ops:
  2.4 74.0 %copy-start.5 = (bf16[768,256]{1,0:T(8,128)(2,1)S(1)}, bf16[768,256]{1,0:T(8,128)(2,1)}, u32[]{:S(2)}) copy-start(bf16[768,256]{1,0:T(8,128)(2,1)} %refs_4_.1) | copy-start | bytes 1179652
  8.0 29.8 %collective-permute-start.4 = (bf16[2048,128]{1,0:T(8,128)(2,1)}, bf16[2048,128]{1,0:T(8,128)(2,1)S(1)}, u32[]{:S(2)}, u32[]{:S(2)}) collective-permute-start(bf16[2048,128]{1,0:T(8,128)(2,1)} %get-tuple-element.35), channel_id=1, source_target_pairs={{0,4},{4,0},{8,12},{12,8},{16,20},{20,16},{24,28},{28,24},{1,5},{5... | collective-permute-start | bytes 1572872 | tf_op jit(solution)/shard_map/ppermute | solution.py:234
  11.0 18.9 %collective-permute-start = (f32[264,256]{1,0:T(8,128)}, f32[264,256]{1,0:T(8,128)}, u32[]{:S(2)}, u32[]{:S(2)}) collective-permute-start(f32[264,256]{1,0:T(8,128)} %get-tuple-element.27), channel_id=1, source_target_pairs={{0,4},{4,0},{8,12},{12,8},{16,20},{20,16},{24,28},{28,24},{1,5},{5... | collective-permute-start | bytes 811016 | tf_op jit(solution)/shard_map/ppermute | solution.py:234
  11.0 79.0 %collective-permute-start.5 = (bf16[2048,128]{1,0:T(8,128)(2,1)}, bf16[2048,128]{1,0:T(8,128)(2,1)S(1)}, u32[]{:S(2)}, u32[]{:S(2)}) collective-permute-start(bf16[2048,128]{1,0:T(8,128)(2,1)} %get-tuple-element.36), channel_id=1, source_target_pairs={{0,4},{4,0},{8,12},{12,8},{16,20},{20,16},{24,28},{28,24},{1,5},{5... | collective-permute-start | bytes 1572872 | tf_op jit(solution)/shard_map/ppermute | solution.py:234
  32.6 11.0 %collective-permute-start.3 = (f32[264,256]{1,0:T(8,128)S(1)}, f32[264,256]{1,0:T(8,128)S(1)}, u32[]{:S(2)}, u32[]{:S(2)}) collective-permute-start(f32[264,256]{1,0:T(8,128)S(1)} %shard_map.147), channel_id=1, source_target_pairs={{0,24},{4,28},{8,0},{12,4},{16,8},{20,12},{24,16},{28,20},{1,25},{... | collective-permute-start | bytes 811016 | tf_op jit(solution)/shard_map/ppermute | solution.py:230
  36.8 38.1 %collective-permute-start.2 = (f32[264,256]{1,0:T(8,128)S(1)}, f32[264,256]{1,0:T(8,128)S(1)}, u32[]{:S(2)}, u32[]{:S(2)}) collective-permute-start(f32[264,256]{1,0:T(8,128)S(1)} %shard_map.147), channel_id=1, source_target_pairs={{0,16},{4,20},{8,24},{12,28},{16,0},{20,4},{24,8},{28,12},{1,17},{... | collective-permute-start | bytes 811016 | tf_op jit(solution)/shard_map/ppermute | solution.py:230
  36.8 43.9 %collective-permute-start.1 = (f32[264,256]{1,0:T(8,128)S(1)}, f32[264,256]{1,0:T(8,128)S(1)}, u32[]{:S(2)}, u32[]{:S(2)}) collective-permute-start(f32[264,256]{1,0:T(8,128)S(1)} %shard_map.147), channel_id=1, source_target_pairs={{0,8},{4,12},{8,16},{12,20},{16,24},{20,28},{24,0},{28,4},{1,9},{5... | collective-permute-start | bytes 811016 | tf_op jit(solution)/shard_map/ppermute | solution.py:230
  37.8 61.6 %collective-permute-start.18 = (bf16[192,2048]{1,0:T(8,128)(2,1)}, bf16[192,2048]{1,0:T(8,128)(2,1)}, u32[]{:S(2)}, u32[]{:S(2)}) collective-permute-start(bf16[192,2048]{1,0:T(8,128)(2,1)} %resid_ref.1), channel_id=1, source_target_pairs={{0,8},{4,12},{8,16},{12,20},{16,24},{20,28},{24,0},{28,4},{1,9},{5... | collective-permute-start | bytes 2359304 | tf_op jit(solution)/shard_map/ppermute | solution.py:230
  43.6 55.1 %collective-permute-start.6 = (bf16[128,2048]{1,0:T(8,128)(2,1)}, bf16[128,2048]{1,0:T(8,128)(2,1)}, u32[]{:S(2)}, u32[]{:S(2)}) collective-permute-start(bf16[128,2048]{1,0:T(8,128)(2,1)} %get-tuple-element.37), channel_id=1, source_target_pairs={{0,4},{4,0},{8,12},{12,8},{16,20},{20,16},{24,28},{28,24},{1,5},{5... | collective-permute-start | bytes 1572872 | tf_op jit(solution)/shard_map/ppermute | solution.py:234
  74.9 24.0 %collective-permute-start.9 = (bf16[128,2048]{1,0:T(8,128)(2,1)}, bf16[128,2048]{1,0:T(8,128)(2,1)}, u32[]{:S(2)}, u32[]{:S(2)}) collective-permute-start(bf16[128,2048]{1,0:T(8,128)(2,1)} %get-tuple-element.40), channel_id=1, source_target_pairs={{0,4},{4,0},{8,12},{12,8},{16,20},{20,16},{24,28},{28,24},{1,5},{5... | collective-permute-start | bytes 1572872 | tf_op jit(solution)/shard_map/ppermute | solution.py:234
  80.7 18.7 %collective-permute-start.7 = (bf16[2048,128]{1,0:T(8,128)(2,1)S(1)}, bf16[2048,128]{1,0:T(8,128)(2,1)}, u32[]{:S(2)}, u32[]{:S(2)}) collective-permute-start(bf16[2048,128]{1,0:T(8,128)(2,1)S(1)} %collective-permute-done.4.refs_5_.refs_7_.refs_4_), channel_id=1, source_target_pairs={{0,2},{1,3},{2,0},{3,1},{4,6},{5,7},{6,4},{7,5},{8,10},{9,11},{10,... | collective-permute-start | bytes 1572872 | tf_op jit(solution)/shard_map/ppermute | solution.py:238
  85.7 27.7 %copy-start.12 = (f32[2048]{0:T(1024)S(1)}, f32[2048]{0:T(1024)}, u32[]{:S(2)}) copy-start(f32[2048]{0:T(1024)} %param.24) | copy-start | bytes 24580
  85.7 11.6 %all-to-all-start = ((bf16[4,192,256]{2,1,0:T(8,128)(2,1)}), bf16[4,192,256]{2,1,0:T(8,128)(2,1)S(1)}, u32[]{:S(2)}, u32[]{:S(2)}) async-start(bf16[4,192,256]{2,1,0:T(8,128)(2,1)} %bitcast.29), calls=%async_computation | async-start | bytes 786432 | tf_op jit(solution)/shard_map/all_to_all | solution.py:547
  90.1 4.7 %collective-permute-start.22 = (bf16[32,192]{1,0:T(8,128)(2,1)S(1)}, bf16[32,192]{1,0:T(8,128)(2,1)S(1)}, u32[]{:S(2)}, u32[]{:S(2)}) collective-permute-start(bf16[32,192]{1,0:T(8,128)(2,1)S(1)} %shard_map.145.route_ref), channel_id=1, source_target_pairs={{0,16},{4,20},{8,24},{12,28},{16,0},{20,4},{24,8},{28,12},{1,17},{... | collective-permute-start | bytes 36872 | tf_op jit(solution)/shard_map/ppermute | solution.py:230
  95.4 13.2 %collective-permute-start.8 = (bf16[2048,128]{1,0:T(8,128)(2,1)S(1)}, bf16[2048,128]{1,0:T(8,128)(2,1)}, u32[]{:S(2)}, u32[]{:S(2)}) collective-permute-start(bf16[2048,128]{1,0:T(8,128)(2,1)S(1)} %collective-permute-done.5.refs_6_.refs_8_.refs_5_), channel_id=1, source_target_pairs={{0,2},{1,3},{2,0},{3,1},{4,6},{5,7},{6,4},{7,5},{8,10},{9,11},{10,... | collective-permute-start | bytes 1572872 | tf_op jit(solution)/shard_map/ppermute | solution.py:238
  98.8 14.1 %collective-permute-start.10 = (bf16[2048,128]{1,0:T(8,128)(2,1)S(1)}, bf16[2048,128]{1,0:T(8,128)(2,1)S(1)}, u32[]{:S(2)}, u32[]{:S(2)}) collective-permute-start(bf16[2048,128]{1,0:T(8,128)(2,1)S(1)} %collective-permute-done.4.refs_5_.refs_7_.refs_4_), channel_id=1, source_target_pairs={{0,1},{1,0},{2,3},{3,2},{4,5},{5,4},{6,7},{7,6},{8,9},{9,8},{10,11... | collective-permute-start | bytes 1572872 | tf_op jit(solution)/shard_map/ppermute | solution.py:238
  98.9 14.5 %collective-permute-start.11 = (bf16[2048,128]{1,0:T(8,128)(2,1)S(1)}, bf16[2048,128]{1,0:T(8,128)(2,1)S(1)}, u32[]{:S(2)}, u32[]{:S(2)}) collective-permute-start(bf16[2048,128]{1,0:T(8,128)(2,1)S(1)} %collective-permute-done.5.refs_6_.refs_8_.refs_5_), channel_id=1, source_target_pairs={{0,1},{1,0},{2,3},{3,2},{4,5},{5,4},{6,7},{7,6},{8,9},{9,8},{10,11... | collective-permute-start | bytes 1572872 | tf_op jit(solution)/shard_map/ppermute | solution.py:238
  99.4 13.5 %collective-permute-start.17 = (bf16[192,1024]{1,0:T(8,128)(2,1)S(1)}, bf16[192,1024]{1,0:T(8,128)(2,1)S(1)}, u32[]{:S(2)}, u32[]{:S(2)}) collective-permute-start(bf16[192,1024]{1,0:T(8,128)(2,1)S(1)} %shard_map.150.gated_ref), channel_id=1, source_target_pairs={{0,8},{4,12},{8,16},{12,20},{16,24},{20,28},{24,0},{28,4},{1,9},{5... | collective-permute-start | bytes 1179656 | tf_op jit(solution)/shard_map/ppermute | solution.py:230
  99.4 14.1 %collective-permute-start.12 = (bf16[128,2048]{1,0:T(8,128)(2,1)}, bf16[128,2048]{1,0:T(8,128)(2,1)S(1)}, u32[]{:S(2)}, u32[]{:S(2)}) collective-permute-start(bf16[128,2048]{1,0:T(8,128)(2,1)} %collective-permute-done.6.refs_7_.refs_9_.refs_6_), channel_id=1, source_target_pairs={{0,1},{1,0},{2,3},{3,2},{4,5},{5,4},{6,7},{7,6},{8,9},{9,8},{10,11... | collective-permute-start | bytes 1572872 | tf_op jit(solution)/shard_map/ppermute | solution.py:238
  108.6 22.6 %collective-permute-start.24 = (bf16[192,2048]{1,0:T(8,128)(2,1)}, bf16[192,2048]{1,0:T(8,128)(2,1)S(1)}, u32[]{:S(2)}, u32[]{:S(2)}) collective-permute-start(bf16[192,2048]{1,0:T(8,128)(2,1)} %collective-permute-done.18.refs_1_), channel_id=1, source_target_pairs={{0,8},{4,12},{8,16},{12,20},{16,24},{20,28},{24,0},{28,4},{1,9},{5... | collective-permute-start | bytes 2359304 | tf_op jit(solution)/shard_map/ppermute | solution.py:230
  112.8 4.0 %collective-permute-start.15 = (bf16[128,2048]{1,0:T(8,128)(2,1)}, bf16[128,2048]{1,0:T(8,128)(2,1)S(1)}, u32[]{:S(2)}, u32[]{:S(2)}) collective-permute-start(bf16[128,2048]{1,0:T(8,128)(2,1)} %collective-permute-done.9.refs_10_.refs_12_.refs_9_), channel_id=1, source_target_pairs={{0,1},{1,0},{2,3},{3,2},{4,5},{5,4},{6,7},{7,6},{8,9},{9,8},{10,11... | collective-permute-start | bytes 1572872 | tf_op jit(solution)/shard_map/ppermute | solution.py:238
  112.8 7.9 %collective-permute-start.13 = (bf16[2048,128]{1,0:T(8,128)(2,1)}, bf16[2048,128]{1,0:T(8,128)(2,1)S(1)}, u32[]{:S(2)}, u32[]{:S(2)}) collective-permute-start(bf16[2048,128]{1,0:T(8,128)(2,1)} %collective-permute-done.7.refs_8_.refs_10_.refs_7_), channel_id=1, source_target_pairs={{0,1},{1,0},{2,3},{3,2},{4,5},{5,4},{6,7},{7,6},{8,9},{9,8},{10,11... | collective-permute-start | bytes 1572872 | tf_op jit(solution)/shard_map/ppermute | solution.py:238
  113.3 17.9 %collective-permute-start.14 = (bf16[2048,128]{1,0:T(8,128)(2,1)}, bf16[2048,128]{1,0:T(8,128)(2,1)S(1)}, u32[]{:S(2)}, u32[]{:S(2)}) collective-permute-start(bf16[2048,128]{1,0:T(8,128)(2,1)} %collective-permute-done.8.refs_9_.refs_11_.refs_8_), channel_id=1, source_target_pairs={{0,1},{1,0},{2,3},{3,2},{4,5},{5,4},{6,7},{7,6},{8,9},{9,8},{10,11... | collective-permute-start | bytes 1572872 | tf_op jit(solution)/shard_map/ppermute | solution.py:238
  113.4 26.1 %collective-permute-start.23 = (bf16[192,1024]{1,0:T(8,128)(2,1)S(1)}, bf16[192,1024]{1,0:T(8,128)(2,1)S(1)}, u32[]{:S(2)}, u32[]{:S(2)}) collective-permute-start(bf16[192,1024]{1,0:T(8,128)(2,1)S(1)} %collective-permute-done.17.refs_0_), channel_id=1, source_target_pairs={{0,8},{4,12},{8,16},{12,20},{16,24},{20,28},{24,0},{28,4},{1,9},{5... | collective-permute-start | bytes 1179656 | tf_op jit(solution)/shard_map/ppermute | solution.py:230
  115.6 23.9 %copy-start.2 = (bf16[1,2048,512]{2,1,0:T(8,128)(2,1)S(1)}, bf16[1,2048,512]{2,1,0:T(8,128)(2,1)}, u32[]{:S(2)}) copy-start(bf16[1,2048,512]{2,1,0:T(8,128)(2,1)} %param.28) | copy-start | bytes 6291460
  115.6 23.9 %copy-start.17 = (bf16[32,192]{1,0:T(8,128)(2,1)S(1)}, bf16[32,192]{1,0:T(8,128)(2,1)}, u32[]{:S(2)}) copy-start(bf16[32,192]{1,0:T(8,128)(2,1)} %copy-done.16) | copy-start | bytes 36868
  116.8 62.7 %collective-permute-start.21 = (bf16[192,2048]{1,0:T(8,128)(2,1)S(1)}, bf16[192,2048]{1,0:T(8,128)(2,1)S(1)}, u32[]{:S(2)}, u32[]{:S(2)}) collective-permute-start(bf16[192,2048]{1,0:T(8,128)(2,1)S(1)} %get-tuple-element.33.refs_0_), channel_id=1, source_target_pairs={{0,24},{4,28},{8,0},{12,4},{16,8},{20,12},{24,16},{28,20},{1,25},{... | collective-permute-start | bytes 2359304 | tf_op jit(solution)/shard_map/ppermute | solution.py:230
  148.0 36.3 %collective-permute-start.25 = (bf16[192,2048]{1,0:T(8,128)(2,1)S(1)}, bf16[192,2048]{1,0:T(8,128)(2,1)S(1)}, u32[]{:S(2)}, u32[]{:S(2)}) collective-permute-start(bf16[192,2048]{1,0:T(8,128)(2,1)S(1)} %shard_map.155), channel_id=1, source_target_pairs={{0,8},{4,12},{8,16},{12,20},{16,24},{20,28},{24,0},{28,4},{1,9},{5... | collective-permute-start | bytes 2359304 | tf_op jit(solution)/shard_map/ppermute | solution.py:230
  148.3 23.6 %collective-permute-start.16 = (bf16[32,192]{1,0:T(8,128)(2,1)S(1)}, bf16[32,192]{1,0:T(8,128)(2,1)S(1)}, u32[]{:S(2)}, u32[]{:S(2)}) collective-permute-start(bf16[32,192]{1,0:T(8,128)(2,1)S(1)} %copy-done.14), channel_id=1, source_target_pairs={{0,8},{4,12},{8,16},{12,20},{16,24},{20,28},{24,0},{28,4},{1,9},{5... | collective-permute-start | bytes 36872 | tf_op jit(solution)/shard_map/ppermute | solution.py:230
  148.3 31.2 %collective-permute-start.20 = (bf16[32,192]{1,0:T(8,128)(2,1)S(1)}, bf16[32,192]{1,0:T(8,128)(2,1)S(1)}, u32[]{:S(2)}, u32[]{:S(2)}) collective-permute-start(bf16[32,192]{1,0:T(8,128)(2,1)S(1)} %copy-done.14), channel_id=1, source_target_pairs={{0,24},{4,28},{8,0},{12,4},{16,8},{20,12},{24,16},{28,20},{1,25},{... | collective-permute-start | bytes 36872 | tf_op jit(solution)/shard_map/ppermute | solution.py:230
  179.3 18.2 %collective-permute-start.19 = (bf16[192,2048]{1,0:T(8,128)(2,1)S(1)}, bf16[192,2048]{1,0:T(8,128)(2,1)S(1)}, u32[]{:S(2)}, u32[]{:S(2)}) collective-permute-start(bf16[192,2048]{1,0:T(8,128)(2,1)S(1)} %shard_map.153), channel_id=1, source_target_pairs={{0,24},{4,28},{8,0},{12,4},{16,8},{20,12},{24,16},{28,20},{1,25},{... | collective-permute-start | bytes 2359304 | tf_op jit(solution)/shard_map/ppermute | solution.py:230
  184.6 29.8 %collective-permute-start.26 = (bf16[192,2048]{1,0:T(8,128)(2,1)S(1)}, bf16[192,2048]{1,0:T(8,128)(2,1)S(1)}, u32[]{:S(2)}, u32[]{:S(2)}) collective-permute-start(bf16[192,2048]{1,0:T(8,128)(2,1)S(1)} %add_convert_fusion.1), channel_id=1, source_target_pairs={{0,8},{4,12},{8,16},{12,20},{16,24},{20,28},{24,0},{28,4},{1,9},{5... | collective-permute-start | bytes 2359304 | tf_op jit(solution)/shard_map/ppermute | solution.py:230
  (18 other events, 87.7 us)

commit v2 on v1

--- a/solution.py
+++ b/solution.py
@@ -156,8 +156,8 @@
 
 
 def read_sent(ref):
-    width = ref.shape[1]
-    return (ref[:width, :],) + unpack_aux(ref[width:, :])
+    rows = ref.shape[0] - AUX_ROWS
+    return (ref[:rows, :],) + unpack_aux(ref[rows:, :])
 
 
 def pair_kernel(place_ref, got_ref, mat_ref, aux_ref, send_ref):
@@ -166,9 +166,10 @@
     own, other = read_state(mat_ref, aux_ref), read_sent(got_ref)
     early = [jnp.where(odd, b, a) for a, b in zip(own, other)]
     late = [jnp.where(odd, a, b) for a, b in zip(own, other)]
-    state = merge(early, late)
-    send_ref[:width, :] = state[0]
-    send_ref[width:, :] = pack_aux(*state[1:], width)
+    mat, *rest = merge(early, late)
+    half = width // 2
+    send_ref[:half, :] = jnp.where(odd, mat[half:], mat[:half])
+    send_ref[half:, :] = pack_aux(*rest, width)
 
 
 def read_out(far, q_ref, num_ref, stat_ref, out_ref, chunk):
@@ -194,15 +195,23 @@
     read_out(far, q_ref, num_ref, stat_ref, out_ref, chunk)
 
 
-def finish_pairs_kernel(place_ref, *refs, chunk, far_count):
-    place = place_ref[0]
-    width = refs[0].shape[1]
-    far = (jnp.zeros((width, width), jnp.float32), jnp.zeros((1, width), jnp.float32))
+def far_kernel(place_ref, *refs):
+    gots, (mat_ref, aux_ref) = refs[:-2], refs[-2:]
+    outer = place_ref[0] // 2
+    far = (jnp.zeros(mat_ref.shape, jnp.float32), jnp.zeros((1, mat_ref.shape[1]), jnp.float32))
     far += (jnp.full((1, 1), FLOOR_LOG, jnp.float32), jnp.zeros((1, 1), jnp.float32))
-    for back in range(far_count, 0, -1):
-        far = merge(far, masked(read_sent(refs[back]), place // 2 >= back))
-    far = merge(far, masked(read_sent(refs[0]), place % 2 == 1))
-    read_out(far, *refs[far_count + 1 :], chunk)
+    for back in range(len(gots), 0, -1):
+        far = merge(far, masked(read_sent(gots[back - 1]), outer >= back))
+    write_state(far, mat_ref, aux_ref)
+
+
+def finish_pairs_kernel(place_ref, pair_ref, own_ref, other_ref, aux_ref, q_ref, num_ref, stat_ref, out_ref, *, chunk):
+    odd = place_ref[0] % 2 == 1
+    own, other = own_ref[...], other_ref[...]
+    mat = jnp.concatenate([jnp.where(odd, other, own), jnp.where(odd, own, other)], axis=0)
+    far = (mat, aux_ref[0:1, :], aux_ref[1:2, :1], aux_ref[2:3, :1])
+    far = merge(far, masked(read_sent(pair_ref), odd))
+    read_out(far, q_ref, num_ref, stat_ref, out_ref, chunk)
 
 
 def call(kernel, outs, *args, specs=None, scratch=(), vmem=16, flops=0, **kwargs):
@@ -265,12 +274,21 @@
     if ring_fits():
         place = lax.axis_index("sp").astype(jnp.int32).reshape(1)
         pair = pair_swap(send)
-        slab = call(pair_kernel, sent, place, pair, mat, aux, specs=[SCALAR] + [VECTOR] * 3)[0]
+        half = [((width // 2 + AUX_ROWS, width), f32)]
+        slab = call(pair_kernel, half, place, pair, mat, aux, specs=[SCALAR] + [VECTOR] * 3)[0]
         far_count = lax.axis_size("sp") // 2 - 1
         fars = []
         for back in range(far_count):
             fars.append(ring_shift(slab, back + 1))
-        operands = [pair, *fars, query, num, stat]
+        far_half, far_aux = call(
+            far_kernel,
+            [((width // 2, width), f32), ((8, width), f32)],
+            place,
+            *fars,
+            specs=[SCALAR] + [VECTOR] * far_count,
+        )
+        other_half = pair_swap(far_half)
+        operands = [pair, far_half, other_half, far_aux, query, num, stat]
         rows = call(
             finish_pairs_kernel,
             [((seq_len, width), b16)],
@@ -278,9 +296,8 @@
             *operands,
             specs=[SCALAR] + [VECTOR] * len(operands),
             chunk=chunk,
-            far_count=far_count,
         )[0]
-        return rows, (send, stat, fars, rows)
+        return rows, (send, stat, fars, far_half, rows)
     far_mat = jnp.zeros((width, width), f32)
     far_aux = jnp.where(iota((8, width), 0) == 1, FLOOR_LOG, 0.0)
     places = lax.axis_size("sp")
@@ -412,7 +429,7 @@
     routed = call(
         route_kernel, [((names, rows), jnp.bfloat16)], routes.T, route_scores.T, expert_count=places
     )[0]
-    send, stat, fars, cell_rows = cell_parts
+    send, stat, fars, far_half, cell_rows = cell_parts
     part = w_gate.shape[2] // 4
     quarter = lax.axis_index("tp") % 4
     quarters = [
@@ -423,6 +440,7 @@
     ]
     quarters, _ = lax.optimization_barrier((quarters, send))
     near, cross, far = [], [], []
+    quarters[2:], _ = lax.optimization_barrier((quarters[2:], far_half))
     for index in range(4):
         near.append(pair_swap(quarters[index]))
     for index, token in enumerate((stat, cell_rows)):
@@ -455,7 +473,7 @@
             count=len(weights),
         )[0]
 
-    routed_late, _ = lax.optimization_barrier((routed, stat))
+    routed_late, _ = lax.optimization_barrier((routed, send))
     shares = [routed]
     for back in range(1, RING):
         shares.append(ring_shift(routed_late, back))

time: 216 us -> 192 us (0.89)
  waiting for transfers between devices: 130 us -> 103 us
  starting transfers between devices: 34.4 us -> 39.2 us
    ppermute x5 -> x6, waiting for transfers between devices: 16.9 us -> 2.9 us  [pair_swap(): lax.ppermute(array, 'sp', [(place, place ^ 1) for place in range(lax.axis...]
    ppermute x14, waiting for transfers between devices: 104 us -> 91.2 us  [ring_shift(): lax.ppermute(array, 'sp', [(place, (place + 2 * step) % places) for place...]
    ppermute x14, starting transfers between devices: 17.8 us -> 21.9 us  [ring_shift(): lax.ppermute(array, 'sp', [(place, (place + 2 * step) % places) for place...]
    ppermute x5 -> x6, starting transfers between devices: 8.07 us -> 10.4 us  [pair_swap(): lax.ppermute(array, 'sp', [(place, place ^ 1) for place in range(lax.axis...]
    pallas_call x11 -> x12, Pallas kernels: 33.3 us -> 31.5 us  [call(): pl.pallas_call(functools.partial(kernel, **kwargs), out_shape=[jax.ShapeD...]
    unnamed x44 -> x48, local copies, waits for them, and re-layouts: 11.9 us -> 11.3 us
  transfers between devices with their start and end apart: 28 -> 29, of which waited for: 11 -> 13; matrix products, arithmetic and copies ran while one was open for 0% -> 2% of each run, Pallas kernels for 14% -> 15%
where the time goes in v2:
time: 192 us; the launch traced here: 191 us
  waiting for transfers between devices  103 us (54%)
  starting transfers between devices  39.2 us (20%)
  Pallas kernels  31.5 us (16%)
  local copies, waits for them, and re-layouts  15.8 us (8%)
    ppermute x14, waiting for transfers between devices, ring_shift(): lax.ppermute(array, 'sp', [(place, (place + 2 * step) % places) for place...  91.2 us
    pallas_call x12, Pallas kernels, call(): pl.pallas_call(functools.partial(kernel, **kwargs), out_shape=[jax.ShapeD...  31.5 us
    ppermute x14, starting transfers between devices, ring_shift(): lax.ppermute(array, 'sp', [(place, (place + 2 * step) % places) for place...  21.9 us
    unnamed x48, local copies, waits for them, and re-layouts  11.3 us
    ppermute x6, starting transfers between devices, pair_swap(): lax.ppermute(array, 'sp', [(place, place ^ 1) for place in range(lax.axis...  10.4 us
    ppermute x8, waiting for transfers between devices, side_swap(): lax.ppermute(array, 'tp', [(place, place ^ distance) for place in range(l...  7.68 us
  transfers between devices with their start and end apart: 29, of which 13 were waited for; matrix products, arithmetic and copies ran while one was open for 2% of the time, Pallas kernels for 15%

profile of v2, /device:TPU:0, one launch (start us, length us, event | category | flops | bytes accessed | tf_op | source)
XLA Modules:
  0.0 191.5 jit_solution(608464817566222768)
XLA Ops:
  0.0 3.5 %shard_map.146 = (f32[264,256]{1,0:T(8,128)}, f32[256,256]{1,0:T(8,128)}, f32[8,256]{1,0:T(8,128)}, f32[8,768]{1,0:T(8,128)}) custom-call(bf16[768,256]{1,0:T(8,128)(2,1)} %k_ref.3, bf16[768,256]{1,0:T(8,128)(2,1)} %v_ref.3, f32[1,768]{1,0:T(1,128)} %forget_ref.1, f32[1,768]{1,0:T(1,128)} %input_ref.1), custom_call_target="tpu_custom_call" | custom-call | tf_op jit(solution)/shard_map/pallas_call | solution.py:221
  3.5 3.0 %collective-permute-start = (f32[264,256]{1,0:T(8,128)}, f32[264,256]{1,0:T(8,128)S(1)}, u32[]{:S(2)}, u32[]{:S(2)}) collective-permute-start(f32[264,256]{1,0:T(8,128)} %get-tuple-element.31), channel_id=1, source_target_pairs={{0,4},{4,0},{8,12},{12,8},{16,20},{20,16},{24,28},{28,24},{1,5},{5... | collective-permute-start | bytes 811016 | tf_op jit(solution)/shard_map/ppermute | solution.py:243
  6.5 2.3 %dynamic-slice_bitcast_fusion = (bf16[128,2048]{1,0:T(8,128)(2,1)}, bf16[128,2048]{1,0:T(8,128)(2,1)}) fusion(bf16[1,512,2048]{2,1,0:T(8,128)(2,1)} %param.29, s32[]{:T(128)S(6)} %select_n.17, s32[]{:T(128)S(6)} %select_n.16), kind=kLoop, calls=%fused_computation.2 | loop fusion | bytes 2097160 | tf_op jit(solution)/shard_map/dynamic_slice | solution.py:439
  8.8 2.2 %dynamic-slice_bitcast_fusion.2 = (bf16[2048,128]{1,0:T(8,128)(2,1)}, bf16[2048,128]{1,0:T(8,128)(2,1)}) fusion(bf16[1,2048,512]{2,1,0:T(8,128)(2,1)} %param.28, s32[]{:T(128)S(6)} %select_n.16, bf16[1,2048,512]{2,1,0:T(8,128)(2,1)S(1)} %copy-done.1), kind=kLoop, calls=%fused_computation.4 | loop fusion | bytes 2097156 | tf_op jit(solution)/shard_map/dynamic_slice | solution.py:437
  11.0 2.7 %collective-permute-done.got_ref.pair_ref = f32[264,256]{1,0:T(8,128)S(1)} collective-permute-done((f32[264,256]{1,0:T(8,128)}, f32[264,256]{1,0:T(8,128)S(1)}, u32[]{:S(2)}, u32[]{:S(2)}) %collective-permute-start) | collective-permute-done | bytes 270368 | tf_op jit(solution)/shard_map/ppermute | solution.py:243
  14.9 3.6 %collective-permute-start.3 = (f32[136,256]{1,0:T(8,128)S(1)}, f32[136,256]{1,0:T(8,128)S(1)}, u32[]{:S(2)}, u32[]{:S(2)}) collective-permute-start(f32[136,256]{1,0:T(8,128)S(1)} %shard_map.147), channel_id=1, source_target_pairs={{0,24},{4,28},{8,0},{12,4},{16,8},{20,12},{24,16},{28,20},{1,25},{... | collective-permute-start | bytes 417800 | tf_op jit(solution)/shard_map/ppermute | solution.py:239
  18.6 2.4 %collective-permute-start.6 = (bf16[2048,128]{1,0:T(8,128)(2,1)}, bf16[2048,128]{1,0:T(8,128)(2,1)S(1)}, u32[]{:S(2)}, u32[]{:S(2)}) collective-permute-start(bf16[2048,128]{1,0:T(8,128)(2,1)} %get-tuple-element.42), channel_id=1, source_target_pairs={{0,4},{4,0},{8,12},{12,8},{16,20},{20,16},{24,28},{28,24},{1,5},{5... | collective-permute-start | bytes 1572872 | tf_op jit(solution)/shard_map/ppermute | solution.py:243
  22.6 2.7 %collective-permute-start.1 = (f32[136,256]{1,0:T(8,128)S(1)}, f32[136,256]{1,0:T(8,128)S(1)}, u32[]{:S(2)}, u32[]{:S(2)}) collective-permute-start(f32[136,256]{1,0:T(8,128)S(1)} %shard_map.147), channel_id=1, source_target_pairs={{0,8},{4,12},{8,16},{12,20},{16,24},{20,28},{24,0},{28,4},{1,9},{5... | collective-permute-start | bytes 417800 | tf_op jit(solution)/shard_map/ppermute | solution.py:239
  25.3 22.2 %collective-permute-done.2.refs_1_ = f32[136,256]{1,0:T(8,128)S(1)} collective-permute-done((f32[136,256]{1,0:T(8,128)S(1)}, f32[136,256]{1,0:T(8,128)S(1)}, u32[]{:S(2)}, u32[]{:S(2)}) %collective-permute-start.2) | collective-permute-done | bytes 139296 | tf_op jit(solution)/shard_map/ppermute | solution.py:239
  47.7 3.0 %collective-permute-start.4 = (f32[128,256]{1,0:T(8,128)S(1)}, f32[128,256]{1,0:T(8,128)S(1)}, u32[]{:S(2)}, u32[]{:S(2)}) collective-permute-start(f32[128,256]{1,0:T(8,128)S(1)} %get-tuple-element.34.own_ref), channel_id=1, source_target_pairs={{0,4},{4,0},{8,12},{12,8},{16,20},{20,16},{24,28},{28,24},{1,5},{5... | collective-permute-start | bytes 393224 | tf_op jit(solution)/shard_map/ppermute | solution.py:243
  50.8 1.9 %collective-permute-start.10 = (bf16[128,2048]{1,0:T(8,128)(2,1)}, bf16[128,2048]{1,0:T(8,128)(2,1)}, u32[]{:S(2)}, u32[]{:S(2)}) collective-permute-start(bf16[128,2048]{1,0:T(8,128)(2,1)} %get-tuple-element.48), channel_id=1, source_target_pairs={{0,4},{4,0},{8,12},{12,8},{16,20},{20,16},{24,28},{28,24},{1,5},{5... | collective-permute-start | bytes 1572872 | tf_op jit(solution)/shard_map/ppermute | solution.py:243
  57.2 1.6 shard_map.150
  59.6 3.6 %all-to-all-start = ((bf16[4,192,256]{2,1,0:T(8,128)(2,1)}), bf16[4,192,256]{2,1,0:T(8,128)(2,1)S(1)}, u32[]{:S(2)}, u32[]{:S(2)}) async-start(bf16[4,192,256]{2,1,0:T(8,128)(2,1)} %bitcast.29), calls=%async_computation | async-start | bytes 786432 | tf_op jit(solution)/shard_map/all_to_all | solution.py:565
  64.0 1.9 collective-permute-start.23
  65.8 2.8 %collective-permute-done.23.route_ref = bf16[32,192]{1,0:T(8,128)(2,1)S(1)} collective-permute-done((bf16[32,192]{1,0:T(8,128)(2,1)S(1)}, bf16[32,192]{1,0:T(8,128)(2,1)S(1)}, u32[]{:S(2)}, u32[]{:S(2)}) %collective-permute-start.23) | collective-permute-done | bytes 12320 | tf_op jit(solution)/shard_map/ppermute | solution.py:239
  69.3 2.0 %collective-permute-start.9 = (bf16[2048,128]{1,0:T(8,128)(2,1)S(1)}, bf16[2048,128]{1,0:T(8,128)(2,1)}, u32[]{:S(2)}, u32[]{:S(2)}) collective-permute-start(bf16[2048,128]{1,0:T(8,128)(2,1)S(1)} %collective-permute-done.6.refs_6_.refs_8_.refs_5_), channel_id=1, source_target_pairs={{0,2},{1,3},{2,0},{3,1},{4,6},{5,7},{6,4},{7,5},{8,10},{9,11},{10,... | collective-permute-start | bytes 1572872 | tf_op jit(solution)/shard_map/ppermute | solution.py:247
  75.6 7.7 %collective-permute-done.9.refs_9_.refs_11_.refs_8_ = bf16[2048,128]{1,0:T(8,128)(2,1)} collective-permute-done((bf16[2048,128]{1,0:T(8,128)(2,1)S(1)}, bf16[2048,128]{1,0:T(8,128)(2,1)}, u32[]{:S(2)}, u32[]{:S(2)}) %collective-permute-start.9) | collective-permute-done | bytes 524320 | tf_op jit(solution)/shard_map/ppermute | solution.py:247
  83.3 1.6 collective-permute-start.25
  84.9 3.2 %collective-permute-done.18.refs_0_ = bf16[192,1024]{1,0:T(8,128)(2,1)S(1)} collective-permute-done((bf16[192,1024]{1,0:T(8,128)(2,1)S(1)}, bf16[192,1024]{1,0:T(8,128)(2,1)S(1)}, u32[]{:S(2)}, u32[]{:S(2)}) %collective-permute-start.18) | collective-permute-done | bytes 393248 | tf_op jit(solution)/shard_map/ppermute | solution.py:239
  88.7 2.2 %copy-done.3 = bf16[1024,2048]{1,0:T(8,128)(2,1)S(1)} copy-done((bf16[1024,2048]{1,0:T(8,128)(2,1)S(1)}, bf16[1024,2048]{1,0:T(8,128)(2,1)}, u32[]{:S(2)}) %copy-start.3) | copy-done | bytes 4194328
  92.1 4.0 %collective-permute-start.22 = (bf16[192,2048]{1,0:T(8,128)(2,1)S(1)}, bf16[192,2048]{1,0:T(8,128)(2,1)S(1)}, u32[]{:S(2)}, u32[]{:S(2)}) collective-permute-start(bf16[192,2048]{1,0:T(8,128)(2,1)S(1)} %get-tuple-element.39.refs_0_), channel_id=1, source_target_pairs={{0,24},{4,28},{8,0},{12,4},{16,8},{20,12},{24,16},{28,20},{1,25},{... | collective-permute-start | bytes 2359304 | tf_op jit(solution)/shard_map/ppermute | solution.py:239
  96.1 9.8 %collective-permute-done.25.refs_1_ = bf16[192,2048]{1,0:T(8,128)(2,1)S(1)} collective-permute-done((bf16[192,2048]{1,0:T(8,128)(2,1)}, bf16[192,2048]{1,0:T(8,128)(2,1)S(1)}, u32[]{:S(2)}, u32[]{:S(2)}) %collective-permute-start.25) | collective-permute-done | bytes 786464 | tf_op jit(solution)/shard_map/ppermute | solution.py:239
  105.9 8.3 %collective-permute-done.24.refs_0_ = bf16[192,1024]{1,0:T(8,128)(2,1)S(1)} collective-permute-done((bf16[192,1024]{1,0:T(8,128)(2,1)S(1)}, bf16[192,1024]{1,0:T(8,128)(2,1)S(1)}, u32[]{:S(2)}, u32[]{:S(2)}) %collective-permute-start.24) | collective-permute-done | bytes 393248 | tf_op jit(solution)/shard_map/ppermute | solution.py:239
  114.3 2.2 %copy-done.4 = bf16[1024,2048]{1,0:T(8,128)(2,1)S(1)} copy-done((bf16[1024,2048]{1,0:T(8,128)(2,1)S(1)}, bf16[1024,2048]{1,0:T(8,128)(2,1)}, u32[]{:S(2)}) %copy-start.4) | copy-done | bytes 4194328
  116.4 6.2 %shard_map.156 = bf16[192,2048]{1,0:T(8,128)(2,1)S(1)} custom-call(s32[1]{0:T(128)} %bitcast.place_ref, bf16[32,192]{1,0:T(8,128)(2,1)S(1)} %copy-done.19, bf16[192,1024]{1,0:T(8,128)(2,1)S(1)} %collective-permute-done.24.refs_0_, bf16[192,2048]{1,0:T(8,128)(2,1)S(1)} %collective-permute-done.25.refs_1_, f32[1,2048]{1,0:T(1,128)S(1)} %bitcast.31, ...), custom_call_target="tpu_custom_call" | custom-call | flops 3221225472 | tf_op jit(solution)/shard_map/pallas_call | solution.py:221
  122.8 3.8 %collective-permute-start.21 = (bf16[32,192]{1,0:T(8,128)(2,1)S(1)}, bf16[32,192]{1,0:T(8,128)(2,1)S(1)}, u32[]{:S(2)}, u32[]{:S(2)}) collective-permute-start(bf16[32,192]{1,0:T(8,128)(2,1)S(1)} %copy-done.16), channel_id=1, source_target_pairs={{0,24},{4,28},{8,0},{12,4},{16,8},{20,12},{24,16},{28,20},{1,25},{... | collective-permute-start | bytes 36872 | tf_op jit(solution)/shard_map/ppermute | solution.py:239
  126.6 20.6 %collective-permute-done.17.route_ref = bf16[32,192]{1,0:T(8,128)(2,1)S(1)} collective-permute-done((bf16[32,192]{1,0:T(8,128)(2,1)S(1)}, bf16[32,192]{1,0:T(8,128)(2,1)S(1)}, u32[]{:S(2)}, u32[]{:S(2)}) %collective-permute-start.17) | collective-permute-done | bytes 12320 | tf_op jit(solution)/shard_map/ppermute | solution.py:239
  147.2 7.3 %shard_map.154 = bf16[192,2048]{1,0:T(8,128)(2,1)S(1)} custom-call(s32[1]{0:T(128)} %bitcast.place_ref, bf16[32,192]{1,0:T(8,128)(2,1)S(1)} %collective-permute-done.17.route_ref, bf16[192,1024]{1,0:T(8,128)(2,1)S(1)} %collective-permute-done.18.refs_0_, bf16[192,2048]{1,0:T(8,128)(2,1)} %collective-permute-done.19.refs_1_, f32[1,2048]{1,0:T(1,128)S(1)} %bitcast.32, ...), custom_call_target="tpu_custom_call" | custom-call | flops 3221225472 | tf_op jit(solution)/shard_map/pallas_call | solution.py:221
  155.4 4.8 %shard_map.155 = bf16[192,2048]{1,0:T(8,128)(2,1)S(1)} custom-call(s32[1]{0:T(128)} %bitcast.place_ref, bf16[32,192]{1,0:T(8,128)(2,1)S(1)} %collective-permute-done.21.route_ref, bf16[192,2048]{1,0:T(8,128)(2,1)S(1)} %collective-permute-done.22.refs_0_, bf16[2048,512]{1,0:T(8,128)(2,1)S(1)} %bitcast.23, bf16[2048,512]{1,0:T(8,128)(2,1)S(1)} %bitcast.27, ...), custom_call_target="tpu_custom_call" | custom-call | flops 2415919104 | tf_op jit(solution)/shard_map/pallas_call | solution.py:221
  162.0 4.8 %shard_map.153 = f32[192,2048]{1,0:T(8,128)S(1)} custom-call(s32[1]{0:T(128)} %bitcast.place_ref, bf16[32,192]{1,0:T(8,128)(2,1)S(1)} %copy-done.16, bf16[192,2048]{1,0:T(8,128)(2,1)S(1)} %get-tuple-element.39.refs_0_, f32[192,2048]{1,0:T(8,128)S(1)} %get-tuple-element.40.refs_1_, bf16[2048,512]{1,0:T(8,128)(2,1)S(1)} %bitcast.24, ...), custom_call_target="tpu_custom_call" | custom-call | flops 2415919104 | tf_op jit(solution)/shard_map/pallas_call | solution.py:221
  166.8 6.7 %collective-permute-done.20 = bf16[192,2048]{1,0:T(8,128)(2,1)S(1)} collective-permute-done((bf16[192,2048]{1,0:T(8,128)(2,1)S(1)}, bf16[192,2048]{1,0:T(8,128)(2,1)S(1)}, u32[]{:S(2)}, u32[]{:S(2)}) %collective-permute-start.20) | collective-permute-done | bytes 786464 | tf_op jit(solution)/shard_map/ppermute | solution.py:239
  173.4 16.8 %collective-permute-done.27 = bf16[192,2048]{1,0:T(8,128)(2,1)S(1)} collective-permute-done((bf16[192,2048]{1,0:T(8,128)(2,1)S(1)}, bf16[192,2048]{1,0:T(8,128)(2,1)S(1)}, u32[]{:S(2)}, u32[]{:S(2)}) %collective-permute-start.27) | collective-permute-done | bytes 786464 | tf_op jit(solution)/shard_map/ppermute | solution.py:239
  (90 shorter events, 19.7 us)
Async XLA Ops:
  3.5 10.2 %collective-permute-start = (f32[264,256]{1,0:T(8,128)}, f32[264,256]{1,0:T(8,128)S(1)}, u32[]{:S(2)}, u32[]{:S(2)}) collective-permute-start(f32[264,256]{1,0:T(8,128)} %get-tuple-element.31), channel_id=1, source_target_pairs={{0,4},{4,0},{8,12},{12,8},{16,20},{20,16},{24,28},{28,24},{1,5},{5... | collective-permute-start | bytes 811016 | tf_op jit(solution)/shard_map/ppermute | solution.py:243
  8.8 43.9 %copy-start.5 = (bf16[768,256]{1,0:T(8,128)(2,1)S(1)}, bf16[768,256]{1,0:T(8,128)(2,1)}, u32[]{:S(2)}) copy-start(bf16[768,256]{1,0:T(8,128)(2,1)} %k_ref.3) | copy-start | bytes 1179652
  11.0 39.8 %collective-permute-start.5 = (bf16[2048,128]{1,0:T(8,128)(2,1)}, bf16[2048,128]{1,0:T(8,128)(2,1)S(1)}, u32[]{:S(2)}, u32[]{:S(2)}) collective-permute-start(bf16[2048,128]{1,0:T(8,128)(2,1)} %get-tuple-element.41), channel_id=1, source_target_pairs={{0,4},{4,0},{8,12},{12,8},{16,20},{20,16},{24,28},{28,24},{1,5},{5... | collective-permute-start | bytes 1572872 | tf_op jit(solution)/shard_map/ppermute | solution.py:243
  14.9 7.7 %collective-permute-start.3 = (f32[136,256]{1,0:T(8,128)S(1)}, f32[136,256]{1,0:T(8,128)S(1)}, u32[]{:S(2)}, u32[]{:S(2)}) collective-permute-start(f32[136,256]{1,0:T(8,128)S(1)} %shard_map.147), channel_id=1, source_target_pairs={{0,24},{4,28},{8,0},{12,4},{16,8},{20,12},{24,16},{28,20},{1,25},{... | collective-permute-start | bytes 417800 | tf_op jit(solution)/shard_map/ppermute | solution.py:239
  18.6 38.7 %copy-start.10 = (f32[264,256]{1,0:T(8,128)S(1)}, f32[264,256]{1,0:T(8,128)}, u32[]{:S(2)}) copy-start(f32[264,256]{1,0:T(8,128)} %copy-done.9) | copy-start | bytes 811012
  18.6 45.4 %collective-permute-start.6 = (bf16[2048,128]{1,0:T(8,128)(2,1)}, bf16[2048,128]{1,0:T(8,128)(2,1)S(1)}, u32[]{:S(2)}, u32[]{:S(2)}) collective-permute-start(bf16[2048,128]{1,0:T(8,128)(2,1)} %get-tuple-element.42), channel_id=1, source_target_pairs={{0,4},{4,0},{8,12},{12,8},{16,20},{20,16},{24,28},{28,24},{1,5},{5... | collective-permute-start | bytes 1572872 | tf_op jit(solution)/shard_map/ppermute | solution.py:243
  20.9 53.2 %collective-permute-start.19 = (bf16[192,2048]{1,0:T(8,128)(2,1)}, bf16[192,2048]{1,0:T(8,128)(2,1)}, u32[]{:S(2)}, u32[]{:S(2)}) collective-permute-start(bf16[192,2048]{1,0:T(8,128)(2,1)} %resid_ref.1), channel_id=1, source_target_pairs={{0,8},{4,12},{8,16},{12,20},{16,24},{20,28},{24,0},{28,4},{1,9},{5... | collective-permute-start | bytes 2359304 | tf_op jit(solution)/shard_map/ppermute | solution.py:239
  20.9 26.6 %collective-permute-start.2 = (f32[136,256]{1,0:T(8,128)S(1)}, f32[136,256]{1,0:T(8,128)S(1)}, u32[]{:S(2)}, u32[]{:S(2)}) collective-permute-start(f32[136,256]{1,0:T(8,128)S(1)} %shard_map.147), channel_id=1, source_target_pairs={{0,16},{4,20},{8,24},{12,28},{16,0},{20,4},{24,8},{28,12},{1,17},{... | collective-permute-start | bytes 417800 | tf_op jit(solution)/shard_map/ppermute | solution.py:239
  22.6 24.9 %collective-permute-start.1 = (f32[136,256]{1,0:T(8,128)S(1)}, f32[136,256]{1,0:T(8,128)S(1)}, u32[]{:S(2)}, u32[]{:S(2)}) collective-permute-start(f32[136,256]{1,0:T(8,128)S(1)} %shard_map.147), channel_id=1, source_target_pairs={{0,8},{4,12},{8,16},{12,20},{16,24},{20,28},{24,0},{28,4},{1,9},{5... | collective-permute-start | bytes 417800 | tf_op jit(solution)/shard_map/ppermute | solution.py:239
  47.7 9.3 %collective-permute-start.4 = (f32[128,256]{1,0:T(8,128)S(1)}, f32[128,256]{1,0:T(8,128)S(1)}, u32[]{:S(2)}, u32[]{:S(2)}) collective-permute-start(f32[128,256]{1,0:T(8,128)S(1)} %get-tuple-element.34.own_ref), channel_id=1, source_target_pairs={{0,4},{4,0},{8,12},{12,8},{16,20},{20,16},{24,28},{28,24},{1,5},{5... | collective-permute-start | bytes 393224 | tf_op jit(solution)/shard_map/ppermute | solution.py:243
  50.7 23.5 %collective-permute-start.7 = (bf16[128,2048]{1,0:T(8,128)(2,1)}, bf16[128,2048]{1,0:T(8,128)(2,1)}, u32[]{:S(2)}, u32[]{:S(2)}) collective-permute-start(bf16[128,2048]{1,0:T(8,128)(2,1)} %get-tuple-element.45), channel_id=1, source_target_pairs={{0,4},{4,0},{8,12},{12,8},{16,20},{20,16},{24,28},{28,24},{1,5},{5... | collective-permute-start | bytes 1572872 | tf_op jit(solution)/shard_map/ppermute | solution.py:243
  50.8 24.1 %collective-permute-start.10 = (bf16[128,2048]{1,0:T(8,128)(2,1)}, bf16[128,2048]{1,0:T(8,128)(2,1)}, u32[]{:S(2)}, u32[]{:S(2)}) collective-permute-start(bf16[128,2048]{1,0:T(8,128)(2,1)} %get-tuple-element.48), channel_id=1, source_target_pairs={{0,4},{4,0},{8,12},{12,8},{16,20},{20,16},{24,28},{28,24},{1,5},{5... | collective-permute-start | bytes 1572872 | tf_op jit(solution)/shard_map/ppermute | solution.py:243
  57.0 18.6 %collective-permute-start.8 = (bf16[2048,128]{1,0:T(8,128)(2,1)S(1)}, bf16[2048,128]{1,0:T(8,128)(2,1)}, u32[]{:S(2)}, u32[]{:S(2)}) collective-permute-start(bf16[2048,128]{1,0:T(8,128)(2,1)S(1)} %collective-permute-done.5.refs_5_.refs_7_.refs_4_), channel_id=1, source_target_pairs={{0,2},{1,3},{2,0},{3,1},{4,6},{5,7},{6,4},{7,5},{8,10},{9,11},{10,... | collective-permute-start | bytes 1572872 | tf_op jit(solution)/shard_map/ppermute | solution.py:247
  59.6 29.1 %copy-start.14 = (f32[2048]{0:T(1024)S(1)}, f32[2048]{0:T(1024)}, u32[]{:S(2)}) copy-start(f32[2048]{0:T(1024)} %param.24) | copy-start | bytes 24580
  59.6 13.1 %all-to-all-start = ((bf16[4,192,256]{2,1,0:T(8,128)(2,1)}), bf16[4,192,256]{2,1,0:T(8,128)(2,1)S(1)}, u32[]{:S(2)}, u32[]{:S(2)}) async-start(bf16[4,192,256]{2,1,0:T(8,128)(2,1)} %bitcast.29), calls=%async_computation | async-start | bytes 786432 | tf_op jit(solution)/shard_map/all_to_all | solution.py:565
  64.0 4.7 %collective-permute-start.23 = (bf16[32,192]{1,0:T(8,128)(2,1)S(1)}, bf16[32,192]{1,0:T(8,128)(2,1)S(1)}, u32[]{:S(2)}, u32[]{:S(2)}) collective-permute-start(bf16[32,192]{1,0:T(8,128)(2,1)S(1)} %shard_map.145.route_ref), channel_id=1, source_target_pairs={{0,16},{4,20},{8,24},{12,28},{16,0},{20,4},{24,8},{28,12},{1,17},{... | collective-permute-start | bytes 36872 | tf_op jit(solution)/shard_map/ppermute | solution.py:239
  69.3 14.0 %collective-permute-start.9 = (bf16[2048,128]{1,0:T(8,128)(2,1)S(1)}, bf16[2048,128]{1,0:T(8,128)(2,1)}, u32[]{:S(2)}, u32[]{:S(2)}) collective-permute-start(bf16[2048,128]{1,0:T(8,128)(2,1)S(1)} %collective-permute-done.6.refs_6_.refs_8_.refs_5_), channel_id=1, source_target_pairs={{0,2},{1,3},{2,0},{3,1},{4,6},{5,7},{6,4},{7,5},{8,10},{9,11},{10,... | collective-permute-start | bytes 1572872 | tf_op jit(solution)/shard_map/ppermute | solution.py:247
  74.1 14.0 %collective-permute-start.11 = (bf16[2048,128]{1,0:T(8,128)(2,1)S(1)}, bf16[2048,128]{1,0:T(8,128)(2,1)S(1)}, u32[]{:S(2)}, u32[]{:S(2)}) collective-permute-start(bf16[2048,128]{1,0:T(8,128)(2,1)S(1)} %collective-permute-done.5.refs_5_.refs_7_.refs_4_), channel_id=1, source_target_pairs={{0,1},{1,0},{2,3},{3,2},{4,5},{5,4},{6,7},{7,6},{8,9},{9,8},{10,11... | collective-permute-start | bytes 1572872 | tf_op jit(solution)/shard_map/ppermute | solution.py:247
  74.2 14.4 %collective-permute-start.12 = (bf16[2048,128]{1,0:T(8,128)(2,1)S(1)}, bf16[2048,128]{1,0:T(8,128)(2,1)S(1)}, u32[]{:S(2)}, u32[]{:S(2)}) collective-permute-start(bf16[2048,128]{1,0:T(8,128)(2,1)S(1)} %collective-permute-done.6.refs_6_.refs_8_.refs_5_), channel_id=1, source_target_pairs={{0,1},{1,0},{2,3},{3,2},{4,5},{5,4},{6,7},{7,6},{8,9},{9,8},{10,11... | collective-permute-start | bytes 1572872 | tf_op jit(solution)/shard_map/ppermute | solution.py:247
  74.9 13.2 %collective-permute-start.18 = (bf16[192,1024]{1,0:T(8,128)(2,1)S(1)}, bf16[192,1024]{1,0:T(8,128)(2,1)S(1)}, u32[]{:S(2)}, u32[]{:S(2)}) collective-permute-start(bf16[192,1024]{1,0:T(8,128)(2,1)S(1)} %shard_map.151.gated_ref), channel_id=1, source_target_pairs={{0,8},{4,12},{8,16},{12,20},{16,24},{20,28},{24,0},{28,4},{1,9},{5... | collective-permute-start | bytes 1179656 | tf_op jit(solution)/shard_map/ppermute | solution.py:239
  75.6 13.0 %collective-permute-start.13 = (bf16[128,2048]{1,0:T(8,128)(2,1)}, bf16[128,2048]{1,0:T(8,128)(2,1)S(1)}, u32[]{:S(2)}, u32[]{:S(2)}) collective-permute-start(bf16[128,2048]{1,0:T(8,128)(2,1)} %collective-permute-done.7.refs_7_.refs_9_.refs_6_), channel_id=1, source_target_pairs={{0,1},{1,0},{2,3},{3,2},{4,5},{5,4},{6,7},{7,6},{8,9},{9,8},{10,11... | collective-permute-start | bytes 1572872 | tf_op jit(solution)/shard_map/ppermute | solution.py:247
  83.3 22.6 %collective-permute-start.25 = (bf16[192,2048]{1,0:T(8,128)(2,1)}, bf16[192,2048]{1,0:T(8,128)(2,1)S(1)}, u32[]{:S(2)}, u32[]{:S(2)}) collective-permute-start(bf16[192,2048]{1,0:T(8,128)(2,1)} %collective-permute-done.19.refs_1_), channel_id=1, source_target_pairs={{0,8},{4,12},{8,16},{12,20},{16,24},{20,28},{24,0},{28,4},{1,9},{5... | collective-permute-start | bytes 2359304 | tf_op jit(solution)/shard_map/ppermute | solution.py:239
  88.1 4.0 %collective-permute-start.16 = (bf16[128,2048]{1,0:T(8,128)(2,1)}, bf16[128,2048]{1,0:T(8,128)(2,1)S(1)}, u32[]{:S(2)}, u32[]{:S(2)}) collective-permute-start(bf16[128,2048]{1,0:T(8,128)(2,1)} %collective-permute-done.10.refs_10_.refs_12_.refs_9_), channel_id=1, source_target_pairs={{0,1},{1,0},{2,3},{3,2},{4,5},{5,4},{6,7},{7,6},{8,9},{9,8},{10,11... | collective-permute-start | bytes 1572872 | tf_op jit(solution)/shard_map/ppermute | solution.py:247
  88.1 8.0 %collective-permute-start.14 = (bf16[2048,128]{1,0:T(8,128)(2,1)}, bf16[2048,128]{1,0:T(8,128)(2,1)S(1)}, u32[]{:S(2)}, u32[]{:S(2)}) collective-permute-start(bf16[2048,128]{1,0:T(8,128)(2,1)} %collective-permute-done.8.refs_8_.refs_10_.refs_7_), channel_id=1, source_target_pairs={{0,1},{1,0},{2,3},{3,2},{4,5},{5,4},{6,7},{7,6},{8,9},{9,8},{10,11... | collective-permute-start | bytes 1572872 | tf_op jit(solution)/shard_map/ppermute | solution.py:247
  88.6 17.3 %collective-permute-start.15 = (bf16[2048,128]{1,0:T(8,128)(2,1)}, bf16[2048,128]{1,0:T(8,128)(2,1)S(1)}, u32[]{:S(2)}, u32[]{:S(2)}) collective-permute-start(bf16[2048,128]{1,0:T(8,128)(2,1)} %collective-permute-done.9.refs_9_.refs_11_.refs_8_), channel_id=1, source_target_pairs={{0,1},{1,0},{2,3},{3,2},{4,5},{5,4},{6,7},{7,6},{8,9},{9,8},{10,11... | collective-permute-start | bytes 1572872 | tf_op jit(solution)/shard_map/ppermute | solution.py:247
  88.7 25.6 %collective-permute-start.24 = (bf16[192,1024]{1,0:T(8,128)(2,1)S(1)}, bf16[192,1024]{1,0:T(8,128)(2,1)S(1)}, u32[]{:S(2)}, u32[]{:S(2)}) collective-permute-start(bf16[192,1024]{1,0:T(8,128)(2,1)S(1)} %collective-permute-done.18.refs_0_), channel_id=1, source_target_pairs={{0,8},{4,12},{8,16},{12,20},{16,24},{20,28},{24,0},{28,4},{1,9},{5... | collective-permute-start | bytes 1179656 | tf_op jit(solution)/shard_map/ppermute | solution.py:239
  92.1 63.4 %collective-permute-start.22 = (bf16[192,2048]{1,0:T(8,128)(2,1)S(1)}, bf16[192,2048]{1,0:T(8,128)(2,1)S(1)}, u32[]{:S(2)}, u32[]{:S(2)}) collective-permute-start(bf16[192,2048]{1,0:T(8,128)(2,1)S(1)} %get-tuple-element.39.refs_0_), channel_id=1, source_target_pairs={{0,24},{4,28},{8,0},{12,4},{16,8},{20,12},{24,16},{28,20},{1,25},{... | collective-permute-start | bytes 2359304 | tf_op jit(solution)/shard_map/ppermute | solution.py:239
  122.6 37.6 %collective-permute-start.26 = (bf16[192,2048]{1,0:T(8,128)(2,1)S(1)}, bf16[192,2048]{1,0:T(8,128)(2,1)S(1)}, u32[]{:S(2)}, u32[]{:S(2)}) collective-permute-start(bf16[192,2048]{1,0:T(8,128)(2,1)S(1)} %shard_map.156), channel_id=1, source_target_pairs={{0,8},{4,12},{8,16},{12,20},{16,24},{20,28},{24,0},{28,4},{1,9},{5... | collective-permute-start | bytes 2359304 | tf_op jit(solution)/shard_map/ppermute | solution.py:239
  122.7 24.5 %collective-permute-start.17 = (bf16[32,192]{1,0:T(8,128)(2,1)S(1)}, bf16[32,192]{1,0:T(8,128)(2,1)S(1)}, u32[]{:S(2)}, u32[]{:S(2)}) collective-permute-start(bf16[32,192]{1,0:T(8,128)(2,1)S(1)} %copy-done.16), channel_id=1, source_target_pairs={{0,8},{4,12},{8,16},{12,20},{16,24},{20,28},{24,0},{28,4},{1,9},{5... | collective-permute-start | bytes 36872 | tf_op jit(solution)/shard_map/ppermute | solution.py:239
  122.8 32.7 %collective-permute-start.21 = (bf16[32,192]{1,0:T(8,128)(2,1)S(1)}, bf16[32,192]{1,0:T(8,128)(2,1)S(1)}, u32[]{:S(2)}, u32[]{:S(2)}) collective-permute-start(bf16[32,192]{1,0:T(8,128)(2,1)S(1)} %copy-done.16), channel_id=1, source_target_pairs={{0,24},{4,28},{8,0},{12,4},{16,8},{20,12},{24,16},{28,20},{1,25},{... | collective-permute-start | bytes 36872 | tf_op jit(solution)/shard_map/ppermute | solution.py:239
  154.6 18.9 %collective-permute-start.20 = (bf16[192,2048]{1,0:T(8,128)(2,1)S(1)}, bf16[192,2048]{1,0:T(8,128)(2,1)S(1)}, u32[]{:S(2)}, u32[]{:S(2)}) collective-permute-start(bf16[192,2048]{1,0:T(8,128)(2,1)S(1)} %shard_map.154), channel_id=1, source_target_pairs={{0,24},{4,28},{8,0},{12,4},{16,8},{20,12},{24,16},{28,20},{1,25},{... | collective-permute-start | bytes 2359304 | tf_op jit(solution)/shard_map/ppermute | solution.py:239
  160.5 29.8 %collective-permute-start.27 = (bf16[192,2048]{1,0:T(8,128)(2,1)S(1)}, bf16[192,2048]{1,0:T(8,128)(2,1)S(1)}, u32[]{:S(2)}, u32[]{:S(2)}) collective-permute-start(bf16[192,2048]{1,0:T(8,128)(2,1)S(1)} %add_convert_fusion.1), channel_id=1, source_target_pairs={{0,8},{4,12},{8,16},{12,20},{16,24},{20,28},{24,0},{28,4},{1,9},{5... | collective-permute-start | bytes 2359304 | tf_op jit(solution)/shard_map/ppermute | solution.py:239
  (21 other events, 144.7 us)

commit v3 on v2

--- a/solution.py
+++ b/solution.py
@@ -429,7 +429,7 @@
     routed = call(
         route_kernel, [((names, rows), jnp.bfloat16)], routes.T, route_scores.T, expert_count=places
     )[0]
-    send, stat, fars, far_half, cell_rows = cell_parts
+    send, _, fars, far_half, cell_rows = cell_parts
     part = w_gate.shape[2] // 4
     quarter = lax.axis_index("tp") % 4
     quarters = [
@@ -443,7 +443,7 @@
     quarters[2:], _ = lax.optimization_barrier((quarters[2:], far_half))
     for index in range(4):
         near.append(pair_swap(quarters[index]))
-    for index, token in enumerate((stat, cell_rows)):
+    for index, token in enumerate((send, cell_rows)):
         source, _ = lax.optimization_barrier((near[index], token))
         cross.append(side_swap(source, 2))
     cross.append(near.pop())
@@ -473,7 +473,7 @@
             count=len(weights),
         )[0]
 
-    routed_late, _ = lax.optimization_barrier((routed, send))
+    routed_late, _ = lax.optimization_barrier((routed, cell_rows))
     shares = [routed]
     for back in range(1, RING):
         shares.append(ring_shift(routed_late, back))

time: 192 us -> 194 us (1.010)
    ppermute x6, waiting for transfers between devices: 2.9 us -> 5.04 us  [pair_swap(): lax.ppermute(array, 'sp', [(place, place ^ 1) for place in range(lax.axis...]
  transfers between devices with their start and end apart: 29 -> 29, of which waited for: 13 -> 12; matrix products, arithmetic and copies ran while one was open for 2% -> 2% of each run, Pallas kernels for 15% -> 14%
where the time goes in v3:
time: 194 us
  waiting for transfers between devices  104 us (54%)
  starting transfers between devices  41.1 us (21%)
  Pallas kernels  31.5 us (16%)
  local copies, waits for them, and re-layouts  15.8 us (8%)
    ppermute x14, waiting for transfers between devices, ring_shift(): lax.ppermute(array, 'sp', [(place, (place + 2 * step) % places) for place...  91.3 us
    pallas_call x12, Pallas kernels, call(): pl.pallas_call(functools.partial(kernel, **kwargs), out_shape=[jax.ShapeD...  31.5 us
    ppermute x14, starting transfers between devices, ring_shift(): lax.ppermute(array, 'sp', [(place, (place + 2 * step) % places) for place...  23.4 us
    unnamed x48, local copies, waits for them, and re-layouts  11.3 us
    ppermute x6, starting transfers between devices, pair_swap(): lax.ppermute(array, 'sp', [(place, place ^ 1) for place in range(lax.axis...  10.4 us
    ppermute x8, waiting for transfers between devices, side_swap(): lax.ppermute(array, 'tp', [(place, place ^ distance) for place in range(l...  7.34 us
    ppermute x6, waiting for transfers between devices, pair_swap(): lax.ppermute(array, 'sp', [(place, place ^ 1) for place in range(lax.axis...  5.04 us
  transfers between devices with their start and end apart: 29, of which 12 were waited for; matrix products, arithmetic and copies ran while one was open for 2% of the time, Pallas kernels for 14%

profile of v3, /device:TPU:0, one launch (start us, length us, event | category | flops | bytes accessed | tf_op | source)
XLA Modules:
  0.0 193.8 jit_solution(5318134970844609966)
XLA Ops:
  0.0 3.5 %shard_map.146 = (f32[264,256]{1,0:T(8,128)}, f32[256,256]{1,0:T(8,128)}, f32[8,256]{1,0:T(8,128)}, f32[8,768]{1,0:T(8,128)}) custom-call(bf16[768,256]{1,0:T(8,128)(2,1)} %k_ref.3, bf16[768,256]{1,0:T(8,128)(2,1)} %v_ref.3, f32[1,768]{1,0:T(1,128)} %forget_ref.1, f32[1,768]{1,0:T(1,128)} %input_ref.1), custom_call_target="tpu_custom_call" | custom-call | tf_op jit(solution)/shard_map/pallas_call | solution.py:221
  3.5 3.0 %collective-permute-start = (f32[264,256]{1,0:T(8,128)}, f32[264,256]{1,0:T(8,128)S(1)}, u32[]{:S(2)}, u32[]{:S(2)}) collective-permute-start(f32[264,256]{1,0:T(8,128)} %get-tuple-element.31), channel_id=1, source_target_pairs={{0,4},{4,0},{8,12},{12,8},{16,20},{20,16},{24,28},{28,24},{1,5},{5... | collective-permute-start | bytes 811016 | tf_op jit(solution)/shard_map/ppermute | solution.py:243
  6.5 2.3 %dynamic-slice_bitcast_fusion = (bf16[128,2048]{1,0:T(8,128)(2,1)}, bf16[128,2048]{1,0:T(8,128)(2,1)}) fusion(bf16[1,512,2048]{2,1,0:T(8,128)(2,1)} %param.29, s32[]{:T(128)S(6)} %select_n.17, s32[]{:T(128)S(6)} %select_n.16), kind=kLoop, calls=%fused_computation.2 | loop fusion | bytes 2097160 | tf_op jit(solution)/shard_map/dynamic_slice | solution.py:439
  8.8 2.2 %dynamic-slice_bitcast_fusion.2 = (bf16[2048,128]{1,0:T(8,128)(2,1)}, bf16[2048,128]{1,0:T(8,128)(2,1)}) fusion(bf16[1,2048,512]{2,1,0:T(8,128)(2,1)} %param.28, s32[]{:T(128)S(6)} %select_n.16, bf16[1,2048,512]{2,1,0:T(8,128)(2,1)S(1)} %copy-done.1), kind=kLoop, calls=%fused_computation.4 | loop fusion | bytes 2097156 | tf_op jit(solution)/shard_map/dynamic_slice | solution.py:437
  11.0 2.7 %collective-permute-done.got_ref.pair_ref = f32[264,256]{1,0:T(8,128)S(1)} collective-permute-done((f32[264,256]{1,0:T(8,128)}, f32[264,256]{1,0:T(8,128)S(1)}, u32[]{:S(2)}, u32[]{:S(2)}) %collective-permute-start) | collective-permute-done | bytes 270368 | tf_op jit(solution)/shard_map/ppermute | solution.py:243
  14.9 3.6 %collective-permute-start.3 = (f32[136,256]{1,0:T(8,128)S(1)}, f32[136,256]{1,0:T(8,128)S(1)}, u32[]{:S(2)}, u32[]{:S(2)}) collective-permute-start(f32[136,256]{1,0:T(8,128)S(1)} %shard_map.147), channel_id=1, source_target_pairs={{0,24},{4,28},{8,0},{12,4},{16,8},{20,12},{24,16},{28,20},{1,25},{... | collective-permute-start | bytes 417800 | tf_op jit(solution)/shard_map/ppermute | solution.py:239
  18.6 2.4 %collective-permute-start.6 = (bf16[2048,128]{1,0:T(8,128)(2,1)}, bf16[2048,128]{1,0:T(8,128)(2,1)S(1)}, u32[]{:S(2)}, u32[]{:S(2)}) collective-permute-start(bf16[2048,128]{1,0:T(8,128)(2,1)} %get-tuple-element.42), channel_id=1, source_target_pairs={{0,4},{4,0},{8,12},{12,8},{16,20},{20,16},{24,28},{28,24},{1,5},{5... | collective-permute-start | bytes 1572872 | tf_op jit(solution)/shard_map/ppermute | solution.py:243
  22.6 2.7 %collective-permute-start.1 = (f32[136,256]{1,0:T(8,128)S(1)}, f32[136,256]{1,0:T(8,128)S(1)}, u32[]{:S(2)}, u32[]{:S(2)}) collective-permute-start(f32[136,256]{1,0:T(8,128)S(1)} %shard_map.147), channel_id=1, source_target_pairs={{0,8},{4,12},{8,16},{12,20},{16,24},{20,28},{24,0},{28,4},{1,9},{5... | collective-permute-start | bytes 417800 | tf_op jit(solution)/shard_map/ppermute | solution.py:239
  25.3 22.2 %collective-permute-done.2.refs_1_ = f32[136,256]{1,0:T(8,128)S(1)} collective-permute-done((f32[136,256]{1,0:T(8,128)S(1)}, f32[136,256]{1,0:T(8,128)S(1)}, u32[]{:S(2)}, u32[]{:S(2)}) %collective-permute-start.2) | collective-permute-done | bytes 139296 | tf_op jit(solution)/shard_map/ppermute | solution.py:239
  47.7 3.0 %collective-permute-start.4 = (f32[128,256]{1,0:T(8,128)S(1)}, f32[128,256]{1,0:T(8,128)S(1)}, u32[]{:S(2)}, u32[]{:S(2)}) collective-permute-start(f32[128,256]{1,0:T(8,128)S(1)} %get-tuple-element.34.own_ref), channel_id=1, source_target_pairs={{0,4},{4,0},{8,12},{12,8},{16,20},{20,16},{24,28},{28,24},{1,5},{5... | collective-permute-start | bytes 393224 | tf_op jit(solution)/shard_map/ppermute | solution.py:243
  50.8 1.9 %collective-permute-start.10 = (bf16[128,2048]{1,0:T(8,128)(2,1)}, bf16[128,2048]{1,0:T(8,128)(2,1)}, u32[]{:S(2)}, u32[]{:S(2)}) collective-permute-start(bf16[128,2048]{1,0:T(8,128)(2,1)} %get-tuple-element.48), channel_id=1, source_target_pairs={{0,4},{4,0},{8,12},{12,8},{16,20},{20,16},{24,28},{28,24},{1,5},{5... | collective-permute-start | bytes 1572872 | tf_op jit(solution)/shard_map/ppermute | solution.py:243
  52.7 2.3 %collective-permute-done.4.other_ref = f32[128,256]{1,0:T(8,128)S(1)} collective-permute-done((f32[128,256]{1,0:T(8,128)S(1)}, f32[128,256]{1,0:T(8,128)S(1)}, u32[]{:S(2)}, u32[]{:S(2)}) %collective-permute-start.4) | collective-permute-done | bytes 131104 | tf_op jit(solution)/shard_map/ppermute | solution.py:243
  62.3 3.6 %all-to-all-start = ((bf16[4,192,256]{2,1,0:T(8,128)(2,1)}), bf16[4,192,256]{2,1,0:T(8,128)(2,1)S(1)}, u32[]{:S(2)}, u32[]{:S(2)}) async-start(bf16[4,192,256]{2,1,0:T(8,128)(2,1)} %bitcast.29), calls=%async_computation | async-start | bytes 786432 | tf_op jit(solution)/shard_map/all_to_all | solution.py:565
  68.5 2.9 %collective-permute-done.23.route_ref = bf16[32,192]{1,0:T(8,128)(2,1)S(1)} collective-permute-done((bf16[32,192]{1,0:T(8,128)(2,1)S(1)}, bf16[32,192]{1,0:T(8,128)(2,1)S(1)}, u32[]{:S(2)}, u32[]{:S(2)}) %collective-permute-start.23) | collective-permute-done | bytes 12320 | tf_op jit(solution)/shard_map/ppermute | solution.py:239
  72.0 2.0 %collective-permute-start.9 = (bf16[2048,128]{1,0:T(8,128)(2,1)S(1)}, bf16[2048,128]{1,0:T(8,128)(2,1)}, u32[]{:S(2)}, u32[]{:S(2)}) collective-permute-start(bf16[2048,128]{1,0:T(8,128)(2,1)S(1)} %collective-permute-done.6.refs_6_.refs_8_.refs_5_), channel_id=1, source_target_pairs={{0,2},{1,3},{2,0},{3,1},{4,6},{5,7},{6,4},{7,5},{8,10},{9,11},{10,... | collective-permute-start | bytes 1572872 | tf_op jit(solution)/shard_map/ppermute | solution.py:247
  76.0 1.9 %collective-permute-start.18 = (bf16[192,1024]{1,0:T(8,128)(2,1)S(1)}, bf16[192,1024]{1,0:T(8,128)(2,1)S(1)}, u32[]{:S(2)}, u32[]{:S(2)}) collective-permute-start(bf16[192,1024]{1,0:T(8,128)(2,1)S(1)} %shard_map.151.gated_ref), channel_id=1, source_target_pairs={{0,8},{4,12},{8,16},{12,20},{16,24},{20,28},{24,0},{28,4},{1,9},{5... | collective-permute-start | bytes 1179656 | tf_op jit(solution)/shard_map/ppermute | solution.py:239
  77.9 7.3 %collective-permute-done.9.refs_9_.refs_11_.refs_8_ = bf16[2048,128]{1,0:T(8,128)(2,1)} collective-permute-done((bf16[2048,128]{1,0:T(8,128)(2,1)S(1)}, bf16[2048,128]{1,0:T(8,128)(2,1)}, u32[]{:S(2)}, u32[]{:S(2)}) %collective-permute-start.9) | collective-permute-done | bytes 524320 | tf_op jit(solution)/shard_map/ppermute | solution.py:247
  87.1 2.3 %collective-permute-done.18.refs_0_ = bf16[192,1024]{1,0:T(8,128)(2,1)S(1)} collective-permute-done((bf16[192,1024]{1,0:T(8,128)(2,1)S(1)}, bf16[192,1024]{1,0:T(8,128)(2,1)S(1)}, u32[]{:S(2)}, u32[]{:S(2)}) %collective-permute-start.18) | collective-permute-done | bytes 393248 | tf_op jit(solution)/shard_map/ppermute | solution.py:239
  90.2 2.2 %copy-done.3 = bf16[1024,2048]{1,0:T(8,128)(2,1)S(1)} copy-done((bf16[1024,2048]{1,0:T(8,128)(2,1)S(1)}, bf16[1024,2048]{1,0:T(8,128)(2,1)}, u32[]{:S(2)}) %copy-start.3) | copy-done | bytes 4194328
  93.6 3.9 %collective-permute-start.22 = (bf16[192,2048]{1,0:T(8,128)(2,1)S(1)}, bf16[192,2048]{1,0:T(8,128)(2,1)S(1)}, u32[]{:S(2)}, u32[]{:S(2)}) collective-permute-start(bf16[192,2048]{1,0:T(8,128)(2,1)S(1)} %get-tuple-element.39.refs_0_), channel_id=1, source_target_pairs={{0,24},{4,28},{8,0},{12,4},{16,8},{20,12},{24,16},{28,20},{1,25},{... | collective-permute-start | bytes 2359304 | tf_op jit(solution)/shard_map/ppermute | solution.py:239
  97.5 10.3 %collective-permute-done.25.refs_1_ = bf16[192,2048]{1,0:T(8,128)(2,1)S(1)} collective-permute-done((bf16[192,2048]{1,0:T(8,128)(2,1)}, bf16[192,2048]{1,0:T(8,128)(2,1)S(1)}, u32[]{:S(2)}, u32[]{:S(2)}) %collective-permute-start.25) | collective-permute-done | bytes 786464 | tf_op jit(solution)/shard_map/ppermute | solution.py:239
  107.8 8.3 %collective-permute-done.24.refs_0_ = bf16[192,1024]{1,0:T(8,128)(2,1)S(1)} collective-permute-done((bf16[192,1024]{1,0:T(8,128)(2,1)S(1)}, bf16[192,1024]{1,0:T(8,128)(2,1)S(1)}, u32[]{:S(2)}, u32[]{:S(2)}) %collective-permute-start.24) | collective-permute-done | bytes 393248 | tf_op jit(solution)/shard_map/ppermute | solution.py:239
  116.1 2.2 %copy-done.4 = bf16[1024,2048]{1,0:T(8,128)(2,1)S(1)} copy-done((bf16[1024,2048]{1,0:T(8,128)(2,1)S(1)}, bf16[1024,2048]{1,0:T(8,128)(2,1)}, u32[]{:S(2)}) %copy-start.4) | copy-done | bytes 4194328
  118.3 6.2 %shard_map.156 = bf16[192,2048]{1,0:T(8,128)(2,1)S(1)} custom-call(s32[1]{0:T(128)} %bitcast.place_ref, bf16[32,192]{1,0:T(8,128)(2,1)S(1)} %copy-done.19, bf16[192,1024]{1,0:T(8,128)(2,1)S(1)} %collective-permute-done.24.refs_0_, bf16[192,2048]{1,0:T(8,128)(2,1)S(1)} %collective-permute-done.25.refs_1_, f32[1,2048]{1,0:T(1,128)S(1)} %bitcast.31, ...), custom_call_target="tpu_custom_call" | custom-call | flops 3221225472 | tf_op jit(solution)/shard_map/pallas_call | solution.py:221
  124.7 3.8 %collective-permute-start.21 = (bf16[32,192]{1,0:T(8,128)(2,1)S(1)}, bf16[32,192]{1,0:T(8,128)(2,1)S(1)}, u32[]{:S(2)}, u32[]{:S(2)}) collective-permute-start(bf16[32,192]{1,0:T(8,128)(2,1)S(1)} %copy-done.16), channel_id=1, source_target_pairs={{0,24},{4,28},{8,0},{12,4},{16,8},{20,12},{24,16},{28,20},{1,25},{... | collective-permute-start | bytes 36872 | tf_op jit(solution)/shard_map/ppermute | solution.py:239
  128.5 20.0 %collective-permute-done.17.route_ref = bf16[32,192]{1,0:T(8,128)(2,1)S(1)} collective-permute-done((bf16[32,192]{1,0:T(8,128)(2,1)S(1)}, bf16[32,192]{1,0:T(8,128)(2,1)S(1)}, u32[]{:S(2)}, u32[]{:S(2)}) %collective-permute-start.17) | collective-permute-done | bytes 12320 | tf_op jit(solution)/shard_map/ppermute | solution.py:239
  148.5 7.3 %shard_map.154 = bf16[192,2048]{1,0:T(8,128)(2,1)S(1)} custom-call(s32[1]{0:T(128)} %bitcast.place_ref, bf16[32,192]{1,0:T(8,128)(2,1)S(1)} %collective-permute-done.17.route_ref, bf16[192,1024]{1,0:T(8,128)(2,1)S(1)} %collective-permute-done.18.refs_0_, bf16[192,2048]{1,0:T(8,128)(2,1)} %collective-permute-done.19.refs_1_, f32[1,2048]{1,0:T(1,128)S(1)} %bitcast.32, ...), custom_call_target="tpu_custom_call" | custom-call | flops 3221225472 | tf_op jit(solution)/shard_map/pallas_call | solution.py:221
  155.8 1.9 collective-permute-start.20
  157.7 4.7 %shard_map.155 = bf16[192,2048]{1,0:T(8,128)(2,1)S(1)} custom-call(s32[1]{0:T(128)} %bitcast.place_ref, bf16[32,192]{1,0:T(8,128)(2,1)S(1)} %collective-permute-done.21.route_ref, bf16[192,2048]{1,0:T(8,128)(2,1)S(1)} %collective-permute-done.22.refs_0_, bf16[2048,512]{1,0:T(8,128)(2,1)S(1)} %bitcast.23, bf16[2048,512]{1,0:T(8,128)(2,1)S(1)} %bitcast.27, ...), custom_call_target="tpu_custom_call" | custom-call | flops 2415919104 | tf_op jit(solution)/shard_map/pallas_call | solution.py:221
  163.2 4.8 %shard_map.153 = f32[192,2048]{1,0:T(8,128)S(1)} custom-call(s32[1]{0:T(128)} %bitcast.place_ref, bf16[32,192]{1,0:T(8,128)(2,1)S(1)} %copy-done.16, bf16[192,2048]{1,0:T(8,128)(2,1)S(1)} %get-tuple-element.39.refs_0_, f32[192,2048]{1,0:T(8,128)S(1)} %get-tuple-element.40.refs_1_, bf16[2048,512]{1,0:T(8,128)(2,1)S(1)} %bitcast.24, ...), custom_call_target="tpu_custom_call" | custom-call | flops 2415919104 | tf_op jit(solution)/shard_map/pallas_call | solution.py:221
  168.0 7.7 %collective-permute-done.20 = bf16[192,2048]{1,0:T(8,128)(2,1)S(1)} collective-permute-done((bf16[192,2048]{1,0:T(8,128)(2,1)S(1)}, bf16[192,2048]{1,0:T(8,128)(2,1)S(1)}, u32[]{:S(2)}, u32[]{:S(2)}) %collective-permute-start.20) | collective-permute-done | bytes 786464 | tf_op jit(solution)/shard_map/ppermute | solution.py:239
  175.7 16.9 %collective-permute-done.27 = bf16[192,2048]{1,0:T(8,128)(2,1)S(1)} collective-permute-done((bf16[192,2048]{1,0:T(8,128)(2,1)S(1)}, bf16[192,2048]{1,0:T(8,128)(2,1)S(1)}, u32[]{:S(2)}, u32[]{:S(2)}) %collective-permute-start.27) | collective-permute-done | bytes 786464 | tf_op jit(solution)/shard_map/ppermute | solution.py:239
  (90 shorter events, 21.4 us)
Async XLA Ops:
  3.5 10.2 %collective-permute-start = (f32[264,256]{1,0:T(8,128)}, f32[264,256]{1,0:T(8,128)S(1)}, u32[]{:S(2)}, u32[]{:S(2)}) collective-permute-start(f32[264,256]{1,0:T(8,128)} %get-tuple-element.31), channel_id=1, source_target_pairs={{0,4},{4,0},{8,12},{12,8},{16,20},{20,16},{24,28},{28,24},{1,5},{5... | collective-permute-start | bytes 811016 | tf_op jit(solution)/shard_map/ppermute | solution.py:243
  8.8 46.8 %copy-start.5 = (bf16[768,256]{1,0:T(8,128)(2,1)S(1)}, bf16[768,256]{1,0:T(8,128)(2,1)}, u32[]{:S(2)}) copy-start(bf16[768,256]{1,0:T(8,128)(2,1)} %k_ref.3) | copy-start | bytes 1179652
  11.0 39.8 %collective-permute-start.5 = (bf16[2048,128]{1,0:T(8,128)(2,1)}, bf16[2048,128]{1,0:T(8,128)(2,1)S(1)}, u32[]{:S(2)}, u32[]{:S(2)}) collective-permute-start(bf16[2048,128]{1,0:T(8,128)(2,1)} %get-tuple-element.41), channel_id=1, source_target_pairs={{0,4},{4,0},{8,12},{12,8},{16,20},{20,16},{24,28},{28,24},{1,5},{5... | collective-permute-start | bytes 1572872 | tf_op jit(solution)/shard_map/ppermute | solution.py:243
  14.9 7.7 %collective-permute-start.3 = (f32[136,256]{1,0:T(8,128)S(1)}, f32[136,256]{1,0:T(8,128)S(1)}, u32[]{:S(2)}, u32[]{:S(2)}) collective-permute-start(f32[136,256]{1,0:T(8,128)S(1)} %shard_map.147), channel_id=1, source_target_pairs={{0,24},{4,28},{8,0},{12,4},{16,8},{20,12},{24,16},{28,20},{1,25},{... | collective-permute-start | bytes 417800 | tf_op jit(solution)/shard_map/ppermute | solution.py:239
  18.6 41.3 %copy-start.10 = (f32[264,256]{1,0:T(8,128)S(1)}, f32[264,256]{1,0:T(8,128)}, u32[]{:S(2)}) copy-start(f32[264,256]{1,0:T(8,128)} %copy-done.9) | copy-start | bytes 811012
  18.6 48.1 %collective-permute-start.6 = (bf16[2048,128]{1,0:T(8,128)(2,1)}, bf16[2048,128]{1,0:T(8,128)(2,1)S(1)}, u32[]{:S(2)}, u32[]{:S(2)}) collective-permute-start(bf16[2048,128]{1,0:T(8,128)(2,1)} %get-tuple-element.42), channel_id=1, source_target_pairs={{0,4},{4,0},{8,12},{12,8},{16,20},{20,16},{24,28},{28,24},{1,5},{5... | collective-permute-start | bytes 1572872 | tf_op jit(solution)/shard_map/ppermute | solution.py:243
  20.9 54.4 %collective-permute-start.19 = (bf16[192,2048]{1,0:T(8,128)(2,1)}, bf16[192,2048]{1,0:T(8,128)(2,1)}, u32[]{:S(2)}, u32[]{:S(2)}) collective-permute-start(bf16[192,2048]{1,0:T(8,128)(2,1)} %resid_ref.1), channel_id=1, source_target_pairs={{0,8},{4,12},{8,16},{12,20},{16,24},{20,28},{24,0},{28,4},{1,9},{5... | collective-permute-start | bytes 2359304 | tf_op jit(solution)/shard_map/ppermute | solution.py:239
  20.9 26.6 %collective-permute-start.2 = (f32[136,256]{1,0:T(8,128)S(1)}, f32[136,256]{1,0:T(8,128)S(1)}, u32[]{:S(2)}, u32[]{:S(2)}) collective-permute-start(f32[136,256]{1,0:T(8,128)S(1)} %shard_map.147), channel_id=1, source_target_pairs={{0,16},{4,20},{8,24},{12,28},{16,0},{20,4},{24,8},{28,12},{1,17},{... | collective-permute-start | bytes 417800 | tf_op jit(solution)/shard_map/ppermute | solution.py:239
  22.6 24.9 %collective-permute-start.1 = (f32[136,256]{1,0:T(8,128)S(1)}, f32[136,256]{1,0:T(8,128)S(1)}, u32[]{:S(2)}, u32[]{:S(2)}) collective-permute-start(f32[136,256]{1,0:T(8,128)S(1)} %shard_map.147), channel_id=1, source_target_pairs={{0,8},{4,12},{8,16},{12,20},{16,24},{20,28},{24,0},{28,4},{1,9},{5... | collective-permute-start | bytes 417800 | tf_op jit(solution)/shard_map/ppermute | solution.py:239
  47.7 7.4 %collective-permute-start.4 = (f32[128,256]{1,0:T(8,128)S(1)}, f32[128,256]{1,0:T(8,128)S(1)}, u32[]{:S(2)}, u32[]{:S(2)}) collective-permute-start(f32[128,256]{1,0:T(8,128)S(1)} %get-tuple-element.34.own_ref), channel_id=1, source_target_pairs={{0,4},{4,0},{8,12},{12,8},{16,20},{20,16},{24,28},{28,24},{1,5},{5... | collective-permute-start | bytes 393224 | tf_op jit(solution)/shard_map/ppermute | solution.py:243
  50.7 24.8 %collective-permute-start.7 = (bf16[128,2048]{1,0:T(8,128)(2,1)}, bf16[128,2048]{1,0:T(8,128)(2,1)}, u32[]{:S(2)}, u32[]{:S(2)}) collective-permute-start(bf16[128,2048]{1,0:T(8,128)(2,1)} %get-tuple-element.45), channel_id=1, source_target_pairs={{0,4},{4,0},{8,12},{12,8},{16,20},{20,16},{24,28},{28,24},{1,5},{5... | collective-permute-start | bytes 1572872 | tf_op jit(solution)/shard_map/ppermute | solution.py:243
  50.8 25.2 %collective-permute-start.10 = (bf16[128,2048]{1,0:T(8,128)(2,1)}, bf16[128,2048]{1,0:T(8,128)(2,1)}, u32[]{:S(2)}, u32[]{:S(2)}) collective-permute-start(bf16[128,2048]{1,0:T(8,128)(2,1)} %get-tuple-element.48), channel_id=1, source_target_pairs={{0,4},{4,0},{8,12},{12,8},{16,20},{20,16},{24,28},{28,24},{1,5},{5... | collective-permute-start | bytes 1572872 | tf_op jit(solution)/shard_map/ppermute | solution.py:243
  55.0 22.9 %collective-permute-start.8 = (bf16[2048,128]{1,0:T(8,128)(2,1)S(1)}, bf16[2048,128]{1,0:T(8,128)(2,1)}, u32[]{:S(2)}, u32[]{:S(2)}) collective-permute-start(bf16[2048,128]{1,0:T(8,128)(2,1)S(1)} %collective-permute-done.5.refs_5_.refs_7_.refs_4_), channel_id=1, source_target_pairs={{0,2},{1,3},{2,0},{3,1},{4,6},{5,7},{6,4},{7,5},{8,10},{9,11},{10,... | collective-permute-start | bytes 1572872 | tf_op jit(solution)/shard_map/ppermute | solution.py:247
  62.3 27.9 %copy-start.14 = (f32[2048]{0:T(1024)S(1)}, f32[2048]{0:T(1024)}, u32[]{:S(2)}) copy-start(f32[2048]{0:T(1024)} %param.24) | copy-start | bytes 24580
  62.3 11.6 %all-to-all-start = ((bf16[4,192,256]{2,1,0:T(8,128)(2,1)}), bf16[4,192,256]{2,1,0:T(8,128)(2,1)S(1)}, u32[]{:S(2)}, u32[]{:S(2)}) async-start(bf16[4,192,256]{2,1,0:T(8,128)(2,1)} %bitcast.29), calls=%async_computation | async-start | bytes 786432 | tf_op jit(solution)/shard_map/all_to_all | solution.py:565
  66.7 4.7 %collective-permute-start.23 = (bf16[32,192]{1,0:T(8,128)(2,1)S(1)}, bf16[32,192]{1,0:T(8,128)(2,1)S(1)}, u32[]{:S(2)}, u32[]{:S(2)}) collective-permute-start(bf16[32,192]{1,0:T(8,128)(2,1)S(1)} %shard_map.145.route_ref), channel_id=1, source_target_pairs={{0,16},{4,20},{8,24},{12,28},{16,0},{20,4},{24,8},{28,12},{1,17},{... | collective-permute-start | bytes 36872 | tf_op jit(solution)/shard_map/ppermute | solution.py:239
  72.0 13.2 %collective-permute-start.9 = (bf16[2048,128]{1,0:T(8,128)(2,1)S(1)}, bf16[2048,128]{1,0:T(8,128)(2,1)}, u32[]{:S(2)}, u32[]{:S(2)}) collective-permute-start(bf16[2048,128]{1,0:T(8,128)(2,1)S(1)} %collective-permute-done.6.refs_6_.refs_8_.refs_5_), channel_id=1, source_target_pairs={{0,2},{1,3},{2,0},{3,1},{4,6},{5,7},{6,4},{7,5},{8,10},{9,11},{10,... | collective-permute-start | bytes 1572872 | tf_op jit(solution)/shard_map/ppermute | solution.py:247
  75.4 14.1 %collective-permute-start.11 = (bf16[2048,128]{1,0:T(8,128)(2,1)S(1)}, bf16[2048,128]{1,0:T(8,128)(2,1)S(1)}, u32[]{:S(2)}, u32[]{:S(2)}) collective-permute-start(bf16[2048,128]{1,0:T(8,128)(2,1)S(1)} %collective-permute-done.5.refs_5_.refs_7_.refs_4_), channel_id=1, source_target_pairs={{0,1},{1,0},{2,3},{3,2},{4,5},{5,4},{6,7},{7,6},{8,9},{9,8},{10,11... | collective-permute-start | bytes 1572872 | tf_op jit(solution)/shard_map/ppermute | solution.py:247
  75.5 14.5 %collective-permute-start.12 = (bf16[2048,128]{1,0:T(8,128)(2,1)S(1)}, bf16[2048,128]{1,0:T(8,128)(2,1)S(1)}, u32[]{:S(2)}, u32[]{:S(2)}) collective-permute-start(bf16[2048,128]{1,0:T(8,128)(2,1)S(1)} %collective-permute-done.6.refs_6_.refs_8_.refs_5_), channel_id=1, source_target_pairs={{0,1},{1,0},{2,3},{3,2},{4,5},{5,4},{6,7},{7,6},{8,9},{9,8},{10,11... | collective-permute-start | bytes 1572872 | tf_op jit(solution)/shard_map/ppermute | solution.py:247
  76.0 13.5 %collective-permute-start.18 = (bf16[192,1024]{1,0:T(8,128)(2,1)S(1)}, bf16[192,1024]{1,0:T(8,128)(2,1)S(1)}, u32[]{:S(2)}, u32[]{:S(2)}) collective-permute-start(bf16[192,1024]{1,0:T(8,128)(2,1)S(1)} %shard_map.151.gated_ref), channel_id=1, source_target_pairs={{0,8},{4,12},{8,16},{12,20},{16,24},{20,28},{24,0},{28,4},{1,9},{5... | collective-permute-start | bytes 1179656 | tf_op jit(solution)/shard_map/ppermute | solution.py:239
  77.9 12.1 %collective-permute-start.13 = (bf16[128,2048]{1,0:T(8,128)(2,1)}, bf16[128,2048]{1,0:T(8,128)(2,1)S(1)}, u32[]{:S(2)}, u32[]{:S(2)}) collective-permute-start(bf16[128,2048]{1,0:T(8,128)(2,1)} %collective-permute-done.7.refs_7_.refs_9_.refs_6_), channel_id=1, source_target_pairs={{0,1},{1,0},{2,3},{3,2},{4,5},{5,4},{6,7},{7,6},{8,9},{9,8},{10,11... | collective-permute-start | bytes 1572872 | tf_op jit(solution)/shard_map/ppermute | solution.py:247
  85.2 22.6 %collective-permute-start.25 = (bf16[192,2048]{1,0:T(8,128)(2,1)}, bf16[192,2048]{1,0:T(8,128)(2,1)S(1)}, u32[]{:S(2)}, u32[]{:S(2)}) collective-permute-start(bf16[192,2048]{1,0:T(8,128)(2,1)} %collective-permute-done.19.refs_1_), channel_id=1, source_target_pairs={{0,8},{4,12},{8,16},{12,20},{16,24},{20,28},{24,0},{28,4},{1,9},{5... | collective-permute-start | bytes 2359304 | tf_op jit(solution)/shard_map/ppermute | solution.py:239
  89.4 4.2 %collective-permute-start.16 = (bf16[128,2048]{1,0:T(8,128)(2,1)}, bf16[128,2048]{1,0:T(8,128)(2,1)S(1)}, u32[]{:S(2)}, u32[]{:S(2)}) collective-permute-start(bf16[128,2048]{1,0:T(8,128)(2,1)} %collective-permute-done.10.refs_10_.refs_12_.refs_9_), channel_id=1, source_target_pairs={{0,1},{1,0},{2,3},{3,2},{4,5},{5,4},{6,7},{7,6},{8,9},{9,8},{10,11... | collective-permute-start | bytes 1572872 | tf_op jit(solution)/shard_map/ppermute | solution.py:247
  89.4 8.1 %collective-permute-start.14 = (bf16[2048,128]{1,0:T(8,128)(2,1)}, bf16[2048,128]{1,0:T(8,128)(2,1)S(1)}, u32[]{:S(2)}, u32[]{:S(2)}) collective-permute-start(bf16[2048,128]{1,0:T(8,128)(2,1)} %collective-permute-done.8.refs_8_.refs_10_.refs_7_), channel_id=1, source_target_pairs={{0,1},{1,0},{2,3},{3,2},{4,5},{5,4},{6,7},{7,6},{8,9},{9,8},{10,11... | collective-permute-start | bytes 1572872 | tf_op jit(solution)/shard_map/ppermute | solution.py:247
  89.9 17.8 %collective-permute-start.15 = (bf16[2048,128]{1,0:T(8,128)(2,1)}, bf16[2048,128]{1,0:T(8,128)(2,1)S(1)}, u32[]{:S(2)}, u32[]{:S(2)}) collective-permute-start(bf16[2048,128]{1,0:T(8,128)(2,1)} %collective-permute-done.9.refs_9_.refs_11_.refs_8_), channel_id=1, source_target_pairs={{0,1},{1,0},{2,3},{3,2},{4,5},{5,4},{6,7},{7,6},{8,9},{9,8},{10,11... | collective-permute-start | bytes 1572872 | tf_op jit(solution)/shard_map/ppermute | solution.py:247
  90.0 26.1 %collective-permute-start.24 = (bf16[192,1024]{1,0:T(8,128)(2,1)S(1)}, bf16[192,1024]{1,0:T(8,128)(2,1)S(1)}, u32[]{:S(2)}, u32[]{:S(2)}) collective-permute-start(bf16[192,1024]{1,0:T(8,128)(2,1)S(1)} %collective-permute-done.18.refs_0_), channel_id=1, source_target_pairs={{0,8},{4,12},{8,16},{12,20},{16,24},{20,28},{24,0},{28,4},{1,9},{5... | collective-permute-start | bytes 1179656 | tf_op jit(solution)/shard_map/ppermute | solution.py:239
  93.6 64.1 %collective-permute-start.22 = (bf16[192,2048]{1,0:T(8,128)(2,1)S(1)}, bf16[192,2048]{1,0:T(8,128)(2,1)S(1)}, u32[]{:S(2)}, u32[]{:S(2)}) collective-permute-start(bf16[192,2048]{1,0:T(8,128)(2,1)S(1)} %get-tuple-element.39.refs_0_), channel_id=1, source_target_pairs={{0,24},{4,28},{8,0},{12,4},{16,8},{20,12},{24,16},{28,20},{1,25},{... | collective-permute-start | bytes 2359304 | tf_op jit(solution)/shard_map/ppermute | solution.py:239
  124.5 37.9 %collective-permute-start.26 = (bf16[192,2048]{1,0:T(8,128)(2,1)S(1)}, bf16[192,2048]{1,0:T(8,128)(2,1)S(1)}, u32[]{:S(2)}, u32[]{:S(2)}) collective-permute-start(bf16[192,2048]{1,0:T(8,128)(2,1)S(1)} %shard_map.156), channel_id=1, source_target_pairs={{0,8},{4,12},{8,16},{12,20},{16,24},{20,28},{24,0},{28,4},{1,9},{5... | collective-permute-start | bytes 2359304 | tf_op jit(solution)/shard_map/ppermute | solution.py:239
  124.7 23.8 %collective-permute-start.17 = (bf16[32,192]{1,0:T(8,128)(2,1)S(1)}, bf16[32,192]{1,0:T(8,128)(2,1)S(1)}, u32[]{:S(2)}, u32[]{:S(2)}) collective-permute-start(bf16[32,192]{1,0:T(8,128)(2,1)S(1)} %copy-done.16), channel_id=1, source_target_pairs={{0,8},{4,12},{8,16},{12,20},{16,24},{20,28},{24,0},{28,4},{1,9},{5... | collective-permute-start | bytes 36872 | tf_op jit(solution)/shard_map/ppermute | solution.py:239
  124.7 33.0 %collective-permute-start.21 = (bf16[32,192]{1,0:T(8,128)(2,1)S(1)}, bf16[32,192]{1,0:T(8,128)(2,1)S(1)}, u32[]{:S(2)}, u32[]{:S(2)}) collective-permute-start(bf16[32,192]{1,0:T(8,128)(2,1)S(1)} %copy-done.16), channel_id=1, source_target_pairs={{0,24},{4,28},{8,0},{12,4},{16,8},{20,12},{24,16},{28,20},{1,25},{... | collective-permute-start | bytes 36872 | tf_op jit(solution)/shard_map/ppermute | solution.py:239
  155.8 19.9 %collective-permute-start.20 = (bf16[192,2048]{1,0:T(8,128)(2,1)S(1)}, bf16[192,2048]{1,0:T(8,128)(2,1)S(1)}, u32[]{:S(2)}, u32[]{:S(2)}) collective-permute-start(bf16[192,2048]{1,0:T(8,128)(2,1)S(1)} %shard_map.154), channel_id=1, source_target_pairs={{0,24},{4,28},{8,0},{12,4},{16,8},{20,12},{24,16},{28,20},{1,25},{... | collective-permute-start | bytes 2359304 | tf_op jit(solution)/shard_map/ppermute | solution.py:239
  162.7 29.8 %collective-permute-start.27 = (bf16[192,2048]{1,0:T(8,128)(2,1)S(1)}, bf16[192,2048]{1,0:T(8,128)(2,1)S(1)}, u32[]{:S(2)}, u32[]{:S(2)}) collective-permute-start(bf16[192,2048]{1,0:T(8,128)(2,1)S(1)} %add_convert_fusion.1), channel_id=1, source_target_pairs={{0,8},{4,12},{8,16},{12,20},{16,24},{20,28},{24,0},{28,4},{1,9},{5... | collective-permute-start | bytes 2359304 | tf_op jit(solution)/shard_map/ppermute | solution.py:239
  (21 other events, 144.8 us)
